TPU v7x, 32 devices: a whole 2x2x4 slice. The times are simulated.
32 devices in a mesh: sp: 4 (over y, x), tp: 8 (over z, core).
Axes of the slice: x: 2, y: 2, z: 4, core: 2. Of those that a mesh axis runs over, the one named last changes fastest.
Arguments:
- queries: bfloat16 [4096, 2048], P('sp', 'tp'), may hold values from -160 to 160
- key_heads: bfloat16 [4096, 512], P('sp'), may hold values from -8 to 8
- value_heads: bfloat16 [4096, 512], P('sp'), may hold values from -4 to 4
- sink_logit: float32 [16], P('tp'), may hold values from -2 to 7
- out_weight: bfloat16 [2048, 2048], P('tp'), may hold values from -0.125 to 0.125
- residual: bfloat16 [4096, 2048], P(('sp', 'tp')), may hold values from -6 to 6
- mixer_gain: float32 [2048], replicated, may hold values from 0.1 to 1.9
- expert_gain: float32 [2048], replicated, may hold values from 0.1 to 1.9
- route_group: int32 [4096], P(('sp', 'tp')), may hold values from 0 to 3, as said below
- route_member: int32 [4096, 2], P(('sp', 'tp')), may hold values from 0 to 2, as said below
- route_weight: bfloat16 [4096, 2], P(('sp', 'tp')), may hold values from 0.19921875 to 1
- gate_weight: bfloat16 [12, 2048, 2048], P('sp', None, 'tp'), may hold values from -0.125 to 0.125
- up_weight: bfloat16 [12, 2048, 2048], P('sp', None, 'tp'), may hold values from -0.125 to 0.125
- down_weight: bfloat16 [12, 2048, 2048], P('sp', 'tp'), may hold values from -0.125 to 0.125
Outputs:
- output: bfloat16 [4096, 2048], P(('sp', 'tp'))
Inputs may be any that keep to these rules, and one draw needn't show every extreme that they name: `route_group`: among the tokens of one device, at most 40 name one group; in every draw one group is named by exactly 40 tokens of every device. `route_member`: the two entries of a token are different members of its group.
All inputs are finite; a program needn't handle non-finite values.
Results may differ from a plain program's by a relative error of at most 0.018.
Values may be sent and summed in bfloat16 or wider, within the bound.
A program may use at most 128 MiB of HBM per device.

v0:
```python
import functools

import jax
import jax.numpy as jnp
from jax import lax
from jax.experimental import pallas as pl
from jax.experimental.pallas import tpu as pltpu
from jax.sharding import PartitionSpec as P

HEADS = 16
KV_HEADS = 4
HEAD_DIM = 128
WINDOW = 128
BLOCK = 128
GROUP_EXPERTS = 3


EPS = 1e-06
NEG_BIG = -1e30


def extended(block, sides, width):
    for axis, dim in sides:
        count = lax.axis_size(axis)
        forward = [(i, i + 1) for i in range(count - 1)]
        backward = [(target, source) for source, target in forward]
        low = lax.ppermute(
            lax.slice_in_dim(block, block.shape[dim] - width, None, axis=dim), axis, forward
        )
        high = lax.ppermute(lax.slice_in_dim(block, 0, width, axis=dim), axis, backward)
        block = jnp.concatenate([low, block, high], axis=dim)
    return block


def window_attention(queries, key_heads, value_heads, sink_logit):
    seq_rows = queries.shape[0]
    heads_dev = sink_logit.shape[0]
    key_group = HEADS // KV_HEADS
    key_start = lax.axis_index("tp") * heads_dev // key_group * HEAD_DIM
    key_own = lax.dynamic_slice_in_dim(key_heads, key_start, HEAD_DIM, 1)
    value_own = lax.dynamic_slice_in_dim(value_heads, key_start, HEAD_DIM, 1)
    padded = extended(jnp.stack([key_own, value_own]), (("sp", 1),), WINDOW)
    blocks = seq_rows // BLOCK
    extent = WINDOW // BLOCK
    tile_rows = padded.reshape(2, blocks + 2 * extent, BLOCK, HEAD_DIM)
    key_spans = jnp.concatenate(
        [tile_rows[:, shifted : shifted + blocks] for shifted in range(2 * extent + 1)], axis=2
    )
    offset = lax.axis_index("sp") * seq_rows
    seq_total = seq_rows * lax.axis_size("sp")
    query_pos = offset + jnp.arange(seq_rows, dtype=jnp.int32).reshape(blocks, BLOCK)
    key_pos = (
        offset
        + (jnp.arange(blocks, dtype=jnp.int32) * BLOCK)[:, None]
        + jnp.arange(BLOCK + 2 * WINDOW, dtype=jnp.int32)[None, :]
        - WINDOW
    )
    inside = (
        (jnp.abs(query_pos[:, :, None] - key_pos[:, None, :]) <= WINDOW)
        & (key_pos >= 0)[:, None, :]
        & (key_pos < seq_total)[:, None, :]
    )
    query_blocks = queries.reshape(blocks, BLOCK, heads_dev, HEAD_DIM)
    scores = jnp.einsum(
        "nqhd,nkd->nhqk", query_blocks, key_spans[0], preferred_element_type=jnp.float32
    ) * HEAD_DIM ** (-0.5)
    scores = jnp.where(inside[:, None], scores, NEG_BIG)
    sink_col = sink_logit[None, :, None, None]
    row_top = jnp.maximum(jnp.max(scores, axis=3, keepdims=True), sink_col)
    exp_terms = jnp.exp(scores - row_top)
    row_mass = jnp.sum(exp_terms, axis=3, keepdims=True) + jnp.exp(sink_col - row_top)
    weight = (exp_terms / row_mass).astype(jnp.bfloat16)
    attended = jnp.einsum(
        "nhqk,nkd->nqhd", weight, key_spans[1], preferred_element_type=jnp.float32
    ).astype(jnp.bfloat16)
    return attended.reshape(seq_rows, heads_dev * HEAD_DIM)


CORES = 2
LANES = 128
VMEM_SPEC = pl.BlockSpec(memory_space=pltpu.VMEM)


def places():
    count = lax.axis_size("tp") // CORES
    me = lax.axis_index("tp")
    chip, core = me // CORES, lax.rem(me, CORES)
    up = lax.rem(chip + 1, count) * CORES + core
    down = lax.rem(chip + count - 1, count) * CORES + core
    partner = chip * CORES + 1 - core
    return count, chip, core, (up, down), partner


def greet(neighbours, partner, peers):
    barrier = pltpu.get_barrier_semaphore()
    for target in (*neighbours, partner):
        pl.semaphore_signal(barrier, inc=1, device_id={"tp": target})
    for peer in peers:
        pl.semaphore_signal(barrier, inc=1, device_id={"sp": peer})
    pl.semaphore_wait(barrier, 3 + len(peers))


def column_halves(width):
    low = (width // LANES + 1) // 2 * LANES
    return (pl.ds(0, low), pl.ds(low, width - low)), (low, width - low)


def spread_kernel(send_ref, out_ref, own_sem, swap_send, swap_recv, ring_send, ring_recv, core_send, core_recv):
    count, chip, core, neighbours, partner = places()
    me = lax.axis_index("tp")
    groups = lax.axis_size("sp")
    group = lax.axis_index("sp")
    order = [lax.rem(group + j, groups) for j in range(groups)]
    greet(neighbours, partner, order[1:])
    halves, _ = column_halves(out_ref.shape[3])

    def swap(j):
        return pltpu.make_async_remote_copy(
            src_ref=send_ref.at[order[j]],
            dst_ref=out_ref.at[me, group],
            send_sem=swap_send.at[j],
            recv_sem=swap_recv.at[j],
            device_id={"sp": order[j]},
        )

    def ring(side, step, j, source):
        place = out_ref.at[source, order[j], :, halves[side]]
        return pltpu.make_async_remote_copy(
            src_ref=place,
            dst_ref=place,
            send_sem=ring_send.at[side, step, j],
            recv_sem=ring_recv.at[side, step, j],
            device_id={"tp": neighbours[side]},
        )

    def across(side, step, j, source):
        place = out_ref.at[source, order[j], :, halves[side]]
        return pltpu.make_async_remote_copy(
            src_ref=place,
            dst_ref=place,
            send_sem=core_send.at[side, step, j],
            recv_sem=core_recv.at[side, step, j],
            device_id={"tp": partner},
        )

    def origin(side, step):
        shift = step if side == 1 else count - step
        return lax.rem(chip + shift, count) * CORES + core

    own = pltpu.make_async_copy(send_ref.at[group], out_ref.at[me, group], own_sem)
    own.start()
    for j in range(1, groups):
        swap(j).start()
    arrival = [0] + [groups - j for j in range(1, groups)]
    for j in range(groups):
        if j == 0:
            own.wait()
        else:
            swap(arrival[j]).wait_recv()
        for side in range(2):
            ring(side, 0, j, me).start()
            across(side, 0, j, me).start()
    for step in range(1, count):
        for j in range(groups):
            for side in range(2):
                source = origin(side, step)
                ring(side, step - 1, j, source).wait_recv()
                if step < count - 1:
                    ring(side, step, j, source).start()
                across(side, step, j, source).start()
    for j in range(1, groups):
        swap(j).wait_send()
    for step in range(count):
        for j in range(groups):
            for side in range(2):
                if step < count - 1:
                    ring(side, step, j, me).wait_send()
                across(side, step, j, me).wait()


def spread(send_rows):
    groups, capacity, width = send_rows.shape
    total = lax.axis_size("tp")
    count = total // CORES
    sem = pltpu.SemaphoreType.DMA
    return pl.pallas_call(
        spread_kernel,
        out_shape=jax.ShapeDtypeStruct((total, groups, capacity, width), send_rows.dtype),
        in_specs=[VMEM_SPEC],
        out_specs=VMEM_SPEC,
        scratch_shapes=[
            sem,
            sem((groups,)),
            sem((groups,)),
            sem((2, count, groups)),
            sem((2, count, groups)),
            sem((2, count, groups)),
            sem((2, count, groups)),
        ],
        compiler_params=pltpu.CompilerParams(collective_id=1, has_side_effects=True),
        name="spread",
    )(send_rows)


def gather_sum_kernel(
    home, part_ref, out_ref, pair0, pair1, hold0, hold1, got0, got1, done,
    core_send, core_recv, ring_send, ring_recv, swap_send, swap_recv,
):
    count, chip, core, neighbours, partner = places()
    pieces = part_ref.shape[1]
    groups = lax.axis_size("sp")
    group = lax.axis_index("sp")
    if home:
        order = [lax.rem(group + j, groups) for j in range(groups)]
        order = order[1:] + order[:1]
        peers = order[:-1]
    else:
        order = list(range(pieces))
        peers = []
    greet(neighbours, partner, peers)
    halves, _ = column_halves(part_ref.shape[3])
    pair, hold, got = (pair0, pair1), (hold0, hold1), (got0, got1)

    def target(side, step):
        shift = count - 1 - step if side == 0 else 1 + step
        return lax.rem(chip + shift, count) * CORES

    def across(side, step, j):
        return pltpu.make_async_remote_copy(
            src_ref=part_ref.at[target(side, step) + 1 - core, order[j], :, halves[side]],
            dst_ref=pair[side].at[step, j],
            send_sem=core_send.at[side, step, j],
            recv_sem=core_recv.at[side, step, j],
            device_id={"tp": partner},
        )

    def ring(side, step, j):
        return pltpu.make_async_remote_copy(
            src_ref=hold[side].at[step, j],
            dst_ref=got[side].at[step, j],
            send_sem=ring_send.at[side, step, j],
            recv_sem=ring_recv.at[side, step, j],
            device_id={"tp": neighbours[side]},
        )

    def swap(j):
        return pltpu.make_async_remote_copy(
            src_ref=done.at[j],
            dst_ref=out_ref.at[group],
            send_sem=swap_send.at[j],
            recv_sem=swap_recv.at[j],
            device_id={"sp": order[j]},
        )

    for step in range(count):
        for j in range(pieces):
            for side in range(2):
                across(side, step, j).start()
    for step in range(count):
        for j in range(pieces):
            for side in range(2):
                across(side, step, j).wait_recv()
                value = part_ref[target(side, step) + core, order[j], :, halves[side]].astype(
                    jnp.float32
                ) + pair[side][step, j].astype(jnp.float32)
                if step > 0:
                    ring(side, step - 1, j).wait_recv()
                    value = value + got[side][step - 1, j].astype(jnp.float32)
                if step < count - 1:
                    hold[side][step, j] = value.astype(hold[side].dtype)
                    ring(side, step, j).start()
                elif home and j < pieces - 1:
                    done[j, :, halves[side]] = value.astype(done.dtype)
                else:
                    out_ref[order[j], :, halves[side]] = value.astype(out_ref.dtype)
            if home and step == count - 1 and j < pieces - 1:
                swap(j).start()
    for step in range(count):
        for j in range(pieces):
            for side in range(2):
                across(side, step, j).wait_send()
                if step < count - 1:
                    ring(side, step, j).wait_send()
    if home:
        for j in range(pieces - 1):
            swap(j).wait()


def gather_sum(part, home, out_type, collective_id):
    total, pieces, rows, width = part.shape
    count = total // CORES
    _, widths = column_halves(width)
    sem = pltpu.SemaphoreType.DMA
    kind = part.dtype
    return pl.pallas_call(
        functools.partial(gather_sum_kernel, home),
        out_shape=jax.ShapeDtypeStruct((pieces, rows, width), out_type),
        in_specs=[VMEM_SPEC],
        out_specs=VMEM_SPEC,
        scratch_shapes=[
            *[pltpu.VMEM((count, pieces, rows, w), kind) for w in widths],
            *[pltpu.VMEM((count, pieces, rows, w), kind) for w in widths],
            *[pltpu.VMEM((count, pieces, rows, w), kind) for w in widths],
            pltpu.VMEM((pieces, rows, width), kind),
            *[sem((2, count, pieces)) for _ in range(4)],
            sem((pieces,)),
            sem((pieces,)),
        ],
        compiler_params=pltpu.CompilerParams(
            collective_id=collective_id, has_side_effects=True
        ),
        name="home_sum" if home else "row_sum",
    )(part)


def experts_kernel(rows_ref, gate_ref, up_ref, down_ref, out_ref):
    width = out_ref.shape[1]
    rows = rows_ref[:, :width]
    gates = rows_ref[:, width:].astype(jnp.float32)
    hidden = []
    for member in range(gate_ref.shape[0]):
        gate_pre = jnp.dot(rows, gate_ref[member], preferred_element_type=jnp.float32)
        up_pre = jnp.dot(rows, up_ref[member], preferred_element_type=jnp.float32)
        value = gate_pre / (1.0 + jnp.exp(-gate_pre)) * up_pre * gates[:, member : member + 1]
        hidden.append(value.astype(jnp.bfloat16))
    out_ref[...] = jnp.dot(
        jnp.concatenate(hidden, axis=1), down_ref[...], preferred_element_type=jnp.float32
    ).astype(out_ref.dtype)


def experts(rows, gate_weight, up_weight, down_weight, block):
    total, padded = rows.shape
    members, width, hidden = gate_weight.shape
    return pl.pallas_call(
        experts_kernel,
        out_shape=jax.ShapeDtypeStruct((total, width), rows.dtype),
        grid=(total // block,),
        in_specs=[
            pl.BlockSpec((block, padded), lambda i: (i, 0)),
            pl.BlockSpec((members, width, hidden), lambda i: (0, 0, 0)),
            pl.BlockSpec((members, width, hidden), lambda i: (0, 0, 0)),
            pl.BlockSpec((members * hidden, width), lambda i: (0, 0)),
        ],
        out_specs=pl.BlockSpec((block, width), lambda i: (i, 0)),
        compiler_params=pltpu.CompilerParams(vmem_limit_bytes=48 * 1024 * 1024),
        cost_estimate=pl.CostEstimate(
            flops=6 * total * width * members * hidden,
            bytes_accessed=2 * total * (width + padded) + 6 * members * hidden * width,
            transcendentals=total * members * hidden,
        ),
        name="experts",
    )(rows, gate_weight, up_weight, down_weight.reshape(members * hidden, width))


def per_device(
    queries,
    key_heads,
    value_heads,
    sink_logit,
    out_weight,
    residual,
    mixer_gain,
    expert_gain,
    route_group,
    route_member,
    route_weight,
    gate_weight,
    up_weight,
    down_weight,
):
    attended = window_attention(queries, key_heads, value_heads, sink_logit)
    tok_rows = residual.shape[0]
    width = out_weight.shape[1]
    parts = lax.axis_size("tp")
    pieces = 4 if tok_rows % 64 == 0 else 1
    product = jnp.dot(attended, out_weight, preferred_element_type=jnp.float32).astype(jnp.bfloat16)
    projected = gather_sum(
        product.reshape(parts, pieces, tok_rows // pieces, width), False, jnp.float32, 0
    ).reshape(tok_rows, width)
    proj_scale = lax.rsqrt(jnp.mean(projected * projected, axis=1, keepdims=True) + EPS)
    mixed_rows = (residual.astype(jnp.float32) + mixer_gain * (projected * proj_scale)).astype(
        jnp.bfloat16
    )
    mixed_float = mixed_rows.astype(jnp.float32)
    norm_scale = lax.rsqrt(jnp.mean(mixed_float * mixed_float, axis=1, keepdims=True) + EPS)
    normed = (mixed_float * norm_scale * expert_gain).astype(jnp.bfloat16)
    groups = lax.axis_size("sp")
    capacity = max(2, (5 * tok_rows + 4 * groups - 1) // (4 * groups))
    group_ids = jnp.arange(groups, dtype=jnp.int32)
    chosen = (route_group[:, None] == group_ids[None, :]).astype(jnp.int32)
    group_rank = jnp.sum(chosen * (jnp.cumsum(chosen, axis=0) - 1), axis=1)
    slot_ids = route_group * capacity + group_rank
    placing = (jnp.arange(groups * capacity, dtype=jnp.int32)[:, None] == slot_ids[None, :]).astype(
        jnp.bfloat16
    )
    member_ids = jnp.arange(GROUP_EXPERTS, dtype=jnp.int32)
    token_gates = jnp.sum(
        route_weight.astype(jnp.float32)[:, :, None]
        * (route_member[:, :, None] == member_ids[None, None, :]).astype(jnp.float32),
        axis=1,
    ).astype(jnp.bfloat16)
    tail = jnp.pad(token_gates, ((0, 0), (0, LANES - GROUP_EXPERTS)))
    send_rows = (
        jnp.dot(placing, jnp.concatenate([normed, tail], axis=1), preferred_element_type=jnp.float32)
        .astype(jnp.bfloat16)
        .reshape(groups, capacity, width + LANES)
    )
    pooled = spread(send_rows)
    partial_out = experts(
        pooled.reshape(-1, width + LANES), gate_weight, up_weight, down_weight, 2 * groups * capacity
    )
    returned = gather_sum(
        partial_out.reshape(parts, groups, capacity, width), True, jnp.bfloat16, 2
    )
    expert_out = lax.dot_general(
        placing,
        returned.reshape(groups * capacity, width),
        (((0,), (0,)), ((), ())),
        preferred_element_type=jnp.float32,
    )
    return (mixed_float + expert_out).astype(jnp.bfloat16)


def solution(mesh):
    placed = (
        P("sp", "tp"),
        P("sp", None),
        P("sp", None),
        P("tp"),
        P("tp", None),
        P(("sp", "tp"), None),
        P(),
        P(),
        P(("sp", "tp")),
        P(("sp", "tp"), None),
        P(("sp", "tp"), None),
        P("sp", None, "tp"),
        P("sp", None, "tp"),
        P("sp", "tp", None),
    )
    return jax.shard_map(
        per_device, mesh=mesh, in_specs=placed, out_specs=P(("sp", "tp"), None), check_vma=False
    )
```

profile of v0, /device:TPU:16, one launch (start us, length us, event | category | flops | bytes accessed | tf_op | source)
XLA Modules:
  0.0 205.7 jit_solution(4345059636989611395)
XLA Ops:
  0.0 1.2 dynamic-slice_bitcast_fusion
  1.2 3.4 %collective-permute-start = (bf16[2,128,128]{2,1,0:T(8,128)(2,1)S(1)}, bf16[2,128,128]{2,1,0:T(8,128)(2,1)S(1)}, u32[]{:S(2)}, u32[]{:S(2)}) collective-permute-start(bf16[2,128,128]{2,1,0:T(8,128)(2,1)S(1)} %get-tuple-element.10), channel_id=1, source_target_pairs={{0,8},{8,16},{16,24},{1,9},{9,17},{17,25},{2,10},{10,18},{18,26},{... | collective-permute-start | bytes 196616 | tf_op jit(solution)/shard_map/ppermute | solution.py:27
  4.6 1.3 collective-permute-start.1
  6.1 0.7 convert_element_type.52
  6.7 0.7 fusion.25
  7.6 0.8 select_reduce_fusion
  8.5 0.7 multiply_add_fusion
  9.1 1.9 fusion.4
  11.0 0.7 fusion.30
  11.8 1.2 reshape.159
  13.1 0.4 fusion.37
  13.6 0.6 fusion.2
  14.3 0.8 fusion
  15.2 1.1 fusion.7
  16.6 3.2 %convolution_convert_fusion = bf16[1024,2048]{1,0:T(8,128)(2,1)} fusion(bf16[256,2048]{1,0:T(8,128)(2,1)S(1)} %copy-done, bf16[32,8,8,128]{3,2,1,0:T(8,128)(2,1)S(1)} %bitcast.63), kind=kOutput, calls=%fused_computation | convolution fusion | flops 1075838976 | bytes 5767168 | tf_op jit(solution)/shard_map/dot_general | solution.py:376
  19.9 42.4 %row_sum.1 = f32[4,32,2048]{2,1,0:T(8,128)} custom-call(bf16[8,4,32,2048]{3,2,1,0:T(8,128)(2,1)} %bitcast.59), custom_call_target="tpu_custom_call" | custom-call | tf_op jit(solution)/shard_map/row_sum/pallas_call | solution.py:295
  62.3 1.4 multiply_reduce_fusion
  63.8 1.6 fusion.9
  65.6 1.2 convolution_convert_fusion.1
  66.8 63.0 %spread.1 = bf16[8,4,40,2176]{3,2,1,0:T(8,128)(2,1)} custom-call(bf16[4,40,2176]{2,1,0:T(8,128)(2,1)} %bitcast.65), custom_call_target="tpu_custom_call" | custom-call | tf_op jit(solution)/shard_map/spread/pallas_call | solution.py:186
  129.8 1.9 copy-done.1
  131.7 17.4 %experts.1 = bf16[1280,2048]{1,0:T(8,128)(2,1)} custom-call(bf16[1280,2176]{1,0:T(8,128)(2,1)} %bitcast.61, bf16[3,2048,256]{2,1,0:T(8,128)(2,1)S(1)} %copy-done.1, bf16[3,2048,256]{2,1,0:T(8,128)(2,1)} %up_ref.1, bf16[768,2048]{1,0:T(8,128)(2,1)} %bitcast.66), custom_call_target="tpu_custom_call" | custom-call | flops 12079595520 | bytes 20250624 | tf_op jit(solution)/shard_map/experts/pallas_call | solution.py:334
  149.1 54.4 %home_sum.1 = bf16[4,40,2048]{2,1,0:T(8,128)(2,1)} custom-call(bf16[8,4,40,2048]{3,2,1,0:T(8,128)(2,1)} %bitcast.62), custom_call_target="tpu_custom_call" | custom-call | tf_op jit(solution)/shard_map/home_sum/pallas_call | solution.py:295
  203.4 2.2 %fusion.1 = bf16[128,2048]{1,0:T(8,128)(2,1)} fusion(bf16[160,2048]{1,0:T(8,128)(2,1)} %bitcast.64, bf16[128,2048]{1,0:T(8,128)(2,1)S(1)} %get-tuple-element.6, s32[128]{0:T(128)S(1)} %multiply_add_fusion), kind=kOutput, calls=%fused_computation.7 | convolution fusion | flops 84692992 | bytes 1704448 | tf_op jit(solution)/shard_map/dot_general | solution.py:415
  (29 shorter events, 1.5 us)
Async XLA Ops:
  0.0 16.6 %copy-start = (bf16[256,2048]{1,0:T(8,128)(2,1)S(1)}, bf16[256,2048]{1,0:T(8,128)(2,1)}, u32[]{:S(2)}) copy-start(bf16[256,2048]{1,0:T(8,128)(2,1)} %param.18) | copy-start | bytes 3145732
  1.2 11.8 %collective-permute-start = (bf16[2,128,128]{2,1,0:T(8,128)(2,1)S(1)}, bf16[2,128,128]{2,1,0:T(8,128)(2,1)S(1)}, u32[]{:S(2)}, u32[]{:S(2)}) collective-permute-start(bf16[2,128,128]{2,1,0:T(8,128)(2,1)S(1)} %get-tuple-element.10), channel_id=1, source_target_pairs={{0,8},{8,16},{16,24},{1,9},{9,17},{17,25},{2,10},{10,18},{18,26},{... | collective-permute-start | bytes 196616 | tf_op jit(solution)/shard_map/ppermute | solution.py:27
  4.6 8.4 %collective-permute-start.1 = (bf16[2,128,128]{2,1,0:T(8,128)(2,1)S(1)}, bf16[2,128,128]{2,1,0:T(8,128)(2,1)S(1)}, u32[]{:S(2)}, u32[]{:S(2)}) collective-permute-start(bf16[2,128,128]{2,1,0:T(8,128)(2,1)S(1)} %get-tuple-element.11), channel_id=1, source_target_pairs={{8,0},{16,8},{24,16},{9,1},{17,9},{25,17},{10,2},{18,10},{26,18},{... | collective-permute-start | bytes 196616 | tf_op jit(solution)/shard_map/ppermute | solution.py:30
  13.6 0.7 copy-start.5
  19.8 43.9 %copy-start.2 = (bf16[128,2048]{1,0:T(8,128)(2,1)S(1)}, bf16[128,2048]{1,0:T(8,128)(2,1)}, u32[]{:S(2)}) copy-start(bf16[128,2048]{1,0:T(8,128)(2,1)} %param.19) | copy-start | bytes 1572868
  19.8 43.9 %copy-start.3 = (f32[2048]{0:T(1024)S(1)}, f32[2048]{0:T(1024)}, u32[]{:S(2)}) copy-start(f32[2048]{0:T(1024)} %param.20) | copy-start | bytes 24580
  19.9 45.5 %copy-start.4 = (f32[2048]{0:T(1024)S(1)}, f32[2048]{0:T(1024)}, u32[]{:S(2)}) copy-start(f32[2048]{0:T(1024)} %param.21) | copy-start | bytes 24580
  129.8 1.9 copy-start.1
where the time goes:
time: 208 us; the launch traced here: 206 us
  Pallas kernels  177 us (85%)
  other arithmetic  10.1 us (5%)
  matrix products  8.38 us (4%)
  local copies, waits for them, and re-layouts  5.16 us (2%)
  starting transfers between devices  4.69 us (2%)
    pallas_call x2, Pallas kernels, gather_sum(): pl.pallas_call(functools.partial(gather_sum_kernel, home), out_shape=jax....  96.8 us
    pallas_call x1, Pallas kernels, spread(): pl.pallas_call(spread_kernel, out_shape=jax.ShapeDtypeStruct((total, grou...  63 us
    pallas_call x1, Pallas kernels, experts(): pl.pallas_call(experts_kernel, out_shape=jax.ShapeDtypeStruct((total, wid...  17.4 us
  transfers between devices with their start and end apart: 2, of which 0 were waited for; matrix products, arithmetic and copies ran while one was open for 3% of the time, Pallas kernels for 0%

commit v1 on v0

--- a/solution.py
+++ b/solution.py
@@ -103,103 +103,6 @@
 def column_halves(width):
     low = (width // LANES + 1) // 2 * LANES
     return (pl.ds(0, low), pl.ds(low, width - low)), (low, width - low)
-
-
-def spread_kernel(send_ref, out_ref, own_sem, swap_send, swap_recv, ring_send, ring_recv, core_send, core_recv):
-    count, chip, core, neighbours, partner = places()
-    me = lax.axis_index("tp")
-    groups = lax.axis_size("sp")
-    group = lax.axis_index("sp")
-    order = [lax.rem(group + j, groups) for j in range(groups)]
-    greet(neighbours, partner, order[1:])
-    halves, _ = column_halves(out_ref.shape[3])
-
-    def swap(j):
-        return pltpu.make_async_remote_copy(
-            src_ref=send_ref.at[order[j]],
-            dst_ref=out_ref.at[me, group],
-            send_sem=swap_send.at[j],
-            recv_sem=swap_recv.at[j],
-            device_id={"sp": order[j]},
-        )
-
-    def ring(side, step, j, source):
-        place = out_ref.at[source, order[j], :, halves[side]]
-        return pltpu.make_async_remote_copy(
-            src_ref=place,
-            dst_ref=place,
-            send_sem=ring_send.at[side, step, j],
-            recv_sem=ring_recv.at[side, step, j],
-            device_id={"tp": neighbours[side]},
-        )
-
-    def across(side, step, j, source):
-        place = out_ref.at[source, order[j], :, halves[side]]
-        return pltpu.make_async_remote_copy(
-            src_ref=place,
-            dst_ref=place,
-            send_sem=core_send.at[side, step, j],
-            recv_sem=core_recv.at[side, step, j],
-            device_id={"tp": partner},
-        )
-
-    def origin(side, step):
-        shift = step if side == 1 else count - step
-        return lax.rem(chip + shift, count) * CORES + core
-
-    own = pltpu.make_async_copy(send_ref.at[group], out_ref.at[me, group], own_sem)
-    own.start()
-    for j in range(1, groups):
-        swap(j).start()
-    arrival = [0] + [groups - j for j in range(1, groups)]
-    for j in range(groups):
-        if j == 0:
-            own.wait()
-        else:
-            swap(arrival[j]).wait_recv()
-        for side in range(2):
-            ring(side, 0, j, me).start()
-            across(side, 0, j, me).start()
-    for step in range(1, count):
-        for j in range(groups):
-            for side in range(2):
-                source = origin(side, step)
-                ring(side, step - 1, j, source).wait_recv()
-                if step < count - 1:
-                    ring(side, step, j, source).start()
-                across(side, step, j, source).start()
-    for j in range(1, groups):
-        swap(j).wait_send()
-    for step in range(count):
-        for j in range(groups):
-            for side in range(2):
-                if step < count - 1:
-                    ring(side, step, j, me).wait_send()
-                across(side, step, j, me).wait()
-
-
-def spread(send_rows):
-    groups, capacity, width = send_rows.shape
-    total = lax.axis_size("tp")
-    count = total // CORES
-    sem = pltpu.SemaphoreType.DMA
-    return pl.pallas_call(
-        spread_kernel,
-        out_shape=jax.ShapeDtypeStruct((total, groups, capacity, width), send_rows.dtype),
-        in_specs=[VMEM_SPEC],
-        out_specs=VMEM_SPEC,
-        scratch_shapes=[
-            sem,
-            sem((groups,)),
-            sem((groups,)),
-            sem((2, count, groups)),
-            sem((2, count, groups)),
-            sem((2, count, groups)),
-            sem((2, count, groups)),
-        ],
-        compiler_params=pltpu.CompilerParams(collective_id=1, has_side_effects=True),
-        name="spread",
-    )(send_rows)
 
 
 def gather_sum_kernel(
@@ -313,43 +216,352 @@
     )(part)
 
 
-def experts_kernel(rows_ref, gate_ref, up_ref, down_ref, out_ref):
-    width = out_ref.shape[1]
-    rows = rows_ref[:, :width]
-    gates = rows_ref[:, width:].astype(jnp.float32)
-    hidden = []
-    for member in range(gate_ref.shape[0]):
-        gate_pre = jnp.dot(rows, gate_ref[member], preferred_element_type=jnp.float32)
-        up_pre = jnp.dot(rows, up_ref[member], preferred_element_type=jnp.float32)
-        value = gate_pre / (1.0 + jnp.exp(-gate_pre)) * up_pre * gates[:, member : member + 1]
-        hidden.append(value.astype(jnp.bfloat16))
-    out_ref[...] = jnp.dot(
-        jnp.concatenate(hidden, axis=1), down_ref[...], preferred_element_type=jnp.float32
-    ).astype(out_ref.dtype)
-
-
-def experts(rows, gate_weight, up_weight, down_weight, block):
-    total, padded = rows.shape
+def line_sequence(i, position, length, side):
+    reach = length - 1 - position if side == 0 else position
+    early = i < reach
+    offset = jnp.where(early, i + 1, 2 * reach - i)
+    home = position + offset if side == 0 else position - offset
+    return home, jnp.where(early, 0, 1)
+
+
+def partner_slot(mine, j, groups):
+    total, bit = 0, 1
+    while bit < groups:
+        total = total + lax.rem(mine // bit + j // bit, 2) * bit
+        bit *= 2
+    return total
+
+
+def moe_kernel(
+    send_ref, gate_hbm, up_hbm, down_hbm, out_ref,
+    rows, res, pair, inc, gate_ref, up_ref, down_ref,
+    weight_sem, own_sem, swap_send, swap_recv, line_send, line_recv, core_send, core_recv,
+    pair_send, pair_recv, sum_send, sum_recv, home_send, home_recv,
+):
+    length = lax.axis_size("tp") // CORES
+    tp = lax.axis_index("tp")
+    z, core = tp // CORES, lax.rem(tp, CORES)
+    partner = z * CORES + 1 - core
+    groups = lax.axis_size("sp")
+    group = lax.axis_index("sp")
+    near = groups // 2
+    width = out_ref.shape[2]
+    last = length - 1
+    sides = (
+        (lax.rem(z + length - 1, length) * CORES + core, z > 0),
+        (lax.rem(z + 1, length) * CORES + core, z < last),
+    )
+    peers = [partner_slot(group, j, groups) for j in range(groups)]
+
+    weights = [
+        pltpu.make_async_copy(source, place, weight_sem.at[n])
+        for n, (source, place) in enumerate(
+            ((gate_hbm, gate_ref), (up_hbm, up_ref), (down_hbm, down_ref))
+        )
+    ]
+    for copy in weights:
+        copy.start()
+
+    @pl.when((z == 0) | (z == last))
+    def _():
+        for slot in range(length):
+            @pl.when(slot != last * (z // last))
+            def _():
+                inc[slot] = jnp.zeros_like(inc[slot])
+
+        @pl.when(z == 0)
+        def _():
+            inc[0] = jnp.zeros_like(inc[0])
+
+        @pl.when(z == last)
+        def _():
+            inc[length] = jnp.zeros_like(inc[length])
+
+    greet((sides[0][0], sides[1][0]), partner, peers[1:])
+
+    def swap(j):
+        return pltpu.make_async_remote_copy(
+            src_ref=send_ref.at[peers[j]],
+            dst_ref=rows.at[z * 2 + j // near, core, j % near],
+            send_sem=swap_send.at[j],
+            recv_sem=swap_recv.at[j],
+            device_id={"sp": peers[j]},
+        )
+
+    def line(side, index, j):
+        place = rows.at[index, core, j]
+        return pltpu.make_async_remote_copy(
+            src_ref=place,
+            dst_ref=place,
+            send_sem=line_send.at[side, index, j],
+            recv_sem=line_recv.at[index, j],
+            device_id={"tp": sides[side][0]},
+        )
+
+    def across(index, j):
+        place = rows.at[index, core, j]
+        return pltpu.make_async_remote_copy(
+            src_ref=place,
+            dst_ref=place,
+            send_sem=core_send.at[index, j],
+            recv_sem=core_recv.at[index, j],
+            device_id={"tp": partner},
+        )
+
+    def share(index):
+        return pltpu.make_async_remote_copy(
+            src_ref=res.at[index, 1 - core],
+            dst_ref=pair.at[index],
+            send_sem=pair_send.at[index],
+            recv_sem=pair_recv.at[index],
+            device_id={"tp": partner},
+        )
+
+    def slot_of(side, target):
+        if side == 1:
+            return target
+        return jnp.where(target == z - 1, length, target)
+
+    def add_on(side, target, half, j):
+        slot = slot_of(side, target)
+        return pltpu.make_async_remote_copy(
+            src_ref=res.at[target * 2 + half, core, j],
+            dst_ref=inc.at[slot, half, j],
+            send_sem=sum_send.at[target * 2 + half, j],
+            recv_sem=sum_recv.at[slot, half, j],
+            device_id={"tp": sides[side][0]},
+        )
+
+    def added(slot, half, j):
+        return pltpu.make_async_remote_copy(
+            src_ref=inc.at[slot, half, j],
+            dst_ref=inc.at[slot, half, j],
+            send_sem=sum_send.at[0, j],
+            recv_sem=sum_recv.at[slot, half, j],
+            device_id={"tp": partner},
+        )
+
+    def back(half, j):
+        return pltpu.make_async_remote_copy(
+            src_ref=res.at[z * 2 + half, core, j],
+            dst_ref=out_ref.at[group],
+            send_sem=home_send.at[half * near + j],
+            recv_sem=home_recv.at[half * near + j],
+            device_id={"sp": peers_at(half, j)},
+        )
+
+    def peers_at(half, j):
+        return peers[half * near + j]
+
+    def forward(side, index, j):
+        @pl.when(sides[side][1])
+        def _():
+            line(side, index, j).start()
+
+    own = pltpu.make_async_copy(send_ref.at[group], rows.at[z * 2, core, 0], own_sem)
+    own.start()
+    for j in range(1, groups):
+        swap(j).start()
+    for j in range(near):
+        if j == 0:
+            own.wait()
+        else:
+            swap(j).wait_recv()
+        for side in range(2):
+            forward(side, z * 2, j)
+        across(z * 2, j).start()
+    for j in range(near):
+        swap(near + j).wait_recv()
+        across(z * 2 + 1, j).start()
+    for copy in weights:
+        copy.wait()
+
+    def expert_rows(index):
+        for j in range(near):
+            across(index, j).wait_recv()
+        block = rows[index].reshape(2 * near * rows.shape[3], rows.shape[4])
+        values = block[:, :width]
+        gates = block[:, width:].astype(jnp.float32)
+        hidden = []
+        for member in range(gate_ref.shape[0]):
+            gate_pre = jnp.dot(values, gate_ref[member], preferred_element_type=jnp.float32)
+            up_pre = jnp.dot(values, up_ref[member], preferred_element_type=jnp.float32)
+            value = gate_pre / (1.0 + jnp.exp(-gate_pre)) * up_pre * gates[:, member : member + 1]
+            hidden.append(value.astype(jnp.bfloat16))
+        total = jnp.dot(
+            jnp.concatenate(hidden, axis=1), down_ref[...], preferred_element_type=jnp.float32
+        )
+        res[index] = total.astype(res.dtype).reshape(res.shape[1:])
+        share(index).start()
+
+    def pass_on(side, i):
+        target, half = line_sequence(i, z, length, 1 - side)
+        index = target * 2 + half
+        share(index).wait_recv()
+        for j in range(near):
+            @pl.when(sides[1 - side][1])
+            def _():
+                added(target, half, j).wait_recv()
+            value = (
+                res[index, core, j].astype(jnp.float32)
+                + pair[index, j].astype(jnp.float32)
+                + inc[target, half, j].astype(jnp.float32)
+            )
+            res[index, core, j] = value.astype(res.dtype)
+            add_on(side, target, half, j).start()
+
+    def finish(half):
+        index = z * 2 + half
+        share(index).wait_recv()
+        for j in range(near):
+            @pl.when(z > 0)
+            def _():
+                added(z, half, j).wait_recv()
+
+            @pl.when(z < last)
+            def _():
+                added(length, half, j).wait_recv()
+            value = (
+                res[index, core, j].astype(jnp.float32)
+                + pair[index, j].astype(jnp.float32)
+                + inc[z, half, j].astype(jnp.float32)
+                + inc[length, half, j].astype(jnp.float32)
+            ).astype(res.dtype)
+            if half == 0 and j == 0:
+                out_ref[group] = value
+            else:
+                res[index, core, j] = value
+                back(half, j).start()
+
+    reaches = (last - z, z)
+    lags = tuple(jnp.where(depth == 0, 0, 2 * depth + 1) for depth in (last - z, z))
+
+    def step(k, carry):
+        for j in range(near):
+            for side in range(2):
+                home, half = line_sequence(k, z, length, side)
+
+                @pl.when(k < 2 * reaches[side])
+                def _(side=side, index=home * 2 + half, j=j):
+                    line(side, index, j).wait_recv()
+                    forward(side, index, j)
+                    across(index, j).start()
+
+                @pl.when(k == 2 * reaches[side])
+                def _(side=side, j=j):
+                    forward(side, z * 2 + 1, j)
+        for side in range(2):
+            i = k - lags[side]
+
+            @pl.when((lags[side] > 0) & (i >= 0) & (i < 2 * reaches[1 - side]))
+            def _(side=side, i=i):
+                pass_on(side, i)
+
+        def job(d, inner):
+            home0, half0 = line_sequence(k, z, length, 0)
+            home1, half1 = line_sequence(k, z, length, 1)
+            index = jnp.where(
+                d == 0, home0 * 2 + half0, jnp.where(d == 1, home1 * 2 + half1, z * 2 + k // 2)
+            )
+            live = jnp.where(
+                d == 0, k < 2 * reaches[0],
+                jnp.where(d == 1, k < 2 * reaches[1], (k == 0) | (k == 2)),
+            )
+
+            @pl.when(live)
+            def _():
+                expert_rows(index)
+
+            return inner
+
+        lax.fori_loop(0, 3, job, 0)
+        for side in range(2):
+            @pl.when((lags[side] == 0) & (k < 2 * reaches[1 - side]))
+            def _(side=side):
+                pass_on(side, k)
+
+        @pl.when(k == 2 * jnp.maximum(z, last - z))
+        def _():
+            finish(0)
+
+        return carry
+
+    lax.fori_loop(0, 2 * length - 1, step, 0)
+    finish(1)
+
+    for j in range(1, groups):
+        swap(j).wait_send()
+        back(j // near, j % near).wait()
+
+    def drain(index, carry):
+        home = index // 2
+        for j in range(near):
+            @pl.when((home >= z) & sides[0][1])
+            def _(j=j):
+                line(0, index, j).wait_send()
+
+            @pl.when((home <= z) & sides[1][1])
+            def _(j=j):
+                line(1, index, j).wait_send()
+
+            across(index, j).wait_send()
+
+            @pl.when(home != z)
+            def _(j=j):
+                add_on(1, home, lax.rem(index, 2), j).wait_send()
+        share(index).wait_send()
+        return carry
+
+    lax.fori_loop(0, 2 * length, drain, 0)
+
+
+def moe(send_rows, gate_weight, up_weight, down_weight):
+    groups, capacity, padded = send_rows.shape
     members, width, hidden = gate_weight.shape
+    length = lax.axis_size("tp") // CORES
+    near = groups // 2
+    kind = send_rows.dtype
+    sem = pltpu.SemaphoreType.DMA
+    hbm = pl.BlockSpec(memory_space=pl.ANY)
+    total = 2 * length * groups * capacity
     return pl.pallas_call(
-        experts_kernel,
-        out_shape=jax.ShapeDtypeStruct((total, width), rows.dtype),
-        grid=(total // block,),
-        in_specs=[
-            pl.BlockSpec((block, padded), lambda i: (i, 0)),
-            pl.BlockSpec((members, width, hidden), lambda i: (0, 0, 0)),
-            pl.BlockSpec((members, width, hidden), lambda i: (0, 0, 0)),
-            pl.BlockSpec((members * hidden, width), lambda i: (0, 0)),
+        moe_kernel,
+        out_shape=jax.ShapeDtypeStruct((groups, capacity, width), kind),
+        in_specs=[VMEM_SPEC, hbm, hbm, hbm],
+        out_specs=VMEM_SPEC,
+        scratch_shapes=[
+            pltpu.VMEM((2 * length, 2, near, capacity, padded), kind),
+            pltpu.VMEM((2 * length, 2, near, capacity, width), kind),
+            pltpu.VMEM((2 * length, near, capacity, width), kind),
+            pltpu.VMEM((length + 1, 2, near, capacity, width), kind),
+            pltpu.VMEM((members, width, hidden), kind),
+            pltpu.VMEM((members, width, hidden), kind),
+            pltpu.VMEM((members * hidden, width), kind),
+            sem((3,)),
+            sem,
+            sem((groups,)),
+            sem((groups,)),
+            sem((2, 2 * length, near)),
+            sem((2 * length, near)),
+            sem((2 * length, near)),
+            sem((2 * length, near)),
+            sem((2 * length,)),
+            sem((2 * length,)),
+            sem((2 * length, near)),
+            sem((length + 1, 2, near)),
+            sem((groups,)),
+            sem((groups,)),
         ],
-        out_specs=pl.BlockSpec((block, width), lambda i: (i, 0)),
-        compiler_params=pltpu.CompilerParams(vmem_limit_bytes=48 * 1024 * 1024),
+        compiler_params=pltpu.CompilerParams(
+            collective_id=1, has_side_effects=True, vmem_limit_bytes=62 * 1024 * 1024
+        ),
         cost_estimate=pl.CostEstimate(
             flops=6 * total * width * members * hidden,
-            bytes_accessed=2 * total * (width + padded) + 6 * members * hidden * width,
+            bytes_accessed=6 * members * hidden * width,
             transcendentals=total * members * hidden,
         ),
-        name="experts",
-    )(rows, gate_weight, up_weight, down_weight.reshape(members * hidden, width))
+        name="moe",
+    )(send_rows, gate_weight, up_weight, down_weight.reshape(members * hidden, width))
 
 
 def per_device(
@@ -386,6 +598,7 @@
     normed = (mixed_float * norm_scale * expert_gain).astype(jnp.bfloat16)
     groups = lax.axis_size("sp")
     capacity = max(2, (5 * tok_rows + 4 * groups - 1) // (4 * groups))
+    capacity = (capacity + 7) // 8 * 8
     group_ids = jnp.arange(groups, dtype=jnp.int32)
     chosen = (route_group[:, None] == group_ids[None, :]).astype(jnp.int32)
     group_rank = jnp.sum(chosen * (jnp.cumsum(chosen, axis=0) - 1), axis=1)
@@ -405,13 +618,7 @@
         .astype(jnp.bfloat16)
         .reshape(groups, capacity, width + LANES)
     )
-    pooled = spread(send_rows)
-    partial_out = experts(
-        pooled.reshape(-1, width + LANES), gate_weight, up_weight, down_weight, 2 * groups * capacity
-    )
-    returned = gather_sum(
-        partial_out.reshape(parts, groups, capacity, width), True, jnp.bfloat16, 2
-    )
+    returned = moe(send_rows, gate_weight, up_weight, down_weight)
     expert_out = lax.dot_general(
         placing,
         returned.reshape(groups * capacity, width),

time: 208 us -> 151 us (0.73)
  Pallas kernels: 177 us -> 124 us
    pallas_call x2 -> x1, Pallas kernels: 96.8 us -> 42.4 us  [gather_sum(): pl.pallas_call(functools.partial(gather_sum_kernel, home), out_shape=jax....]
    pallas_call x2 -> x1, Pallas kernels: 80.3 us -> 81.9 us  [moe(): pl.pallas_call(moe_kernel, out_shape=jax.ShapeDtypeStruct((groups, capaci...]
  transfers between devices with their start and end apart: 2 -> 2, of which waited for: 0 -> 0; matrix products, arithmetic and copies ran while one was open for 3% -> 4% of each run, Pallas kernels for 0% -> 0%
where the time goes in v1:
time: 151 us; the launch traced here: 150 us
  Pallas kernels  124 us (82%)
  other arithmetic  9.39 us (6%)
  matrix products  8.35 us (6%)
  starting transfers between devices  4.69 us (3%)
  local copies, waits for them, and re-layouts  3.3 us (2%)
    pallas_call x1, Pallas kernels, moe(): pl.pallas_call(moe_kernel, out_shape=jax.ShapeDtypeStruct((groups, capaci...  81.9 us
    pallas_call x1, Pallas kernels, gather_sum(): pl.pallas_call(functools.partial(gather_sum_kernel, home), out_shape=jax....  42.4 us
    ppermute x1, starting transfers between devices, extended(): lax.ppermute(lax.slice_in_dim(block, block.shape[dim] - width, None, axis...  3.4 us
    dot_general x1, matrix products, per_device(): jnp.dot(attended, out_weight, preferred_element_type=jnp.float32)  3.22 us
  transfers between devices with their start and end apart: 2, of which 0 were waited for; matrix products, arithmetic and copies ran while one was open for 4% of the time, Pallas kernels for 0%

profile of v1, /device:TPU:16, one launch (start us, length us, event | category | flops | bytes accessed | tf_op | source)
XLA Modules:
  0.0 150.3 jit_solution(7711014930342594698)
XLA Ops:
  0.0 1.2 dynamic-slice_bitcast_fusion
  1.2 3.4 %collective-permute-start = (bf16[2,128,128]{2,1,0:T(8,128)(2,1)S(1)}, bf16[2,128,128]{2,1,0:T(8,128)(2,1)S(1)}, u32[]{:S(2)}, u32[]{:S(2)}) collective-permute-start(bf16[2,128,128]{2,1,0:T(8,128)(2,1)S(1)} %get-tuple-element.10), channel_id=1, source_target_pairs={{0,8},{8,16},{16,24},{1,9},{9,17},{17,25},{2,10},{10,18},{18,26},{... | collective-permute-start | bytes 196616 | tf_op jit(solution)/shard_map/ppermute | solution.py:27
  4.6 1.3 collective-permute-start.1
  6.1 1.2 reshape.153
  7.3 0.7 fusion.25
  8.0 0.2 reduce_window_sum.11
  8.2 0.8 select_reduce_fusion
  9.0 0.7 multiply_add_fusion
  9.7 0.7 convert_element_type.52
  10.3 1.9 %fusion.4 = pred[8,128,384]{1,2,0:T(8,128)(4,1)S(1)} fusion(s32[8,384]{1,0:T(8,128)S(1)} %add_add_fusion, s32[8,128]{1,0:T(8,128)S(1)} %add_add_fusion.1, pred[8,384]{1,0:T(8,128)(4,1)S(1)} %get-tuple-element.13, pred[8,384]{1,0:T(8,128)(4,1)S(1)} %get-tuple-element.12), kind=kLoop, calls=%fused_computation.14 | loop fusion | flops 1966080 | bytes 415744 | tf_op jit(solution)/shard_map/and | solution.py:59
  12.4 0.4 fusion.37
  12.8 0.1 pad_maximum_fusion
  12.9 0.6 fusion.2
  13.7 0.8 fusion
  14.5 1.1 fusion.7
  15.6 0.3 copy.34
  16.0 3.2 %convolution_convert_fusion = bf16[1024,2048]{1,0:T(8,128)(2,1)} fusion(bf16[256,2048]{1,0:T(8,128)(2,1)S(1)} %copy-done, bf16[32,8,8,128]{3,2,1,0:T(8,128)(2,1)S(1)} %bitcast.59), kind=kOutput, calls=%fused_computation | convolution fusion | flops 1075838976 | bytes 5767168 | tf_op jit(solution)/shard_map/dot_general | solution.py:588
  19.2 42.4 %row_sum.1 = f32[4,32,2048]{2,1,0:T(8,128)} custom-call(bf16[8,4,32,2048]{3,2,1,0:T(8,128)(2,1)} %bitcast.57), custom_call_target="tpu_custom_call" | custom-call | tf_op jit(solution)/shard_map/row_sum/pallas_call | solution.py:198
  61.6 1.4 multiply_reduce_fusion
  63.1 1.6 %fusion.9 = (f32[128]{0:T(128)S(1)}, bf16[128,2048]{1,0:T(8,128)(2,1)S(1)}) fusion(f32[128]{0:T(128)S(1)} %rsqrt.20, f32[4,32,2048]{2,1,0:T(8,128)} %row_sum.1, f32[2048]{0:T(1024)S(1)} %copy-done.2, bf16[128,2048]{1,0:T(8,128)(2,1)S(1)} %copy-done.1), kind=kLoop, calls=%fused_computation.20 | loop fusion | flops 2097024 | bytes 2106368 | tf_op jit(solution)/shard_map/reduce_sum | solution.py:597
  64.7 0.2 fusion.11
  64.9 1.2 convolution_convert_fusion.1
  66.1 81.9 %moe.1 = bf16[4,40,2048]{2,1,0:T(8,128)(2,1)} custom-call(bf16[4,40,2176]{2,1,0:T(8,128)(2,1)} %bitcast.62, bf16[3,2048,256]{2,1,0:T(8,128)(2,1)} %gate_hbm.1, bf16[3,2048,256]{2,1,0:T(8,128)(2,1)} %up_hbm.1, bf16[768,2048]{1,0:T(8,128)(2,1)} %bitcast.61), custom_call_target="tpu_custom_call" | custom-call | flops 12079595520 | bytes 9437184 | tf_op jit(solution)/shard_map/moe/pallas_call | solution.py:527
  148.1 2.2 %fusion.1 = bf16[128,2048]{1,0:T(8,128)(2,1)} fusion(bf16[160,2048]{1,0:T(8,128)(2,1)} %bitcast.60, bf16[128,2048]{1,0:T(8,128)(2,1)S(1)} %get-tuple-element.6, s32[128]{0:T(128)S(1)} %multiply_add_fusion), kind=kOutput, calls=%fused_computation.7 | convolution fusion | flops 84692992 | bytes 1704448 | tf_op jit(solution)/shard_map/dot_general | solution.py:622
  (27 shorter events, 0.7 us)
Async XLA Ops:
  0.0 15.9 %copy-start = (bf16[256,2048]{1,0:T(8,128)(2,1)S(1)}, bf16[256,2048]{1,0:T(8,128)(2,1)}, u32[]{:S(2)}) copy-start(bf16[256,2048]{1,0:T(8,128)(2,1)} %param.18) | copy-start | bytes 3145732
  0.0 12.2 %copy-start.5 = (s32[128,2]{0,1:T(2,128)S(1)}, s32[128,2]{0,1:T(2,128)}, u32[]{:S(2)}) copy-start(s32[128,2]{0,1:T(2,128)} %param.23) | copy-start | bytes 3076
  1.2 11.2 %collective-permute-start = (bf16[2,128,128]{2,1,0:T(8,128)(2,1)S(1)}, bf16[2,128,128]{2,1,0:T(8,128)(2,1)S(1)}, u32[]{:S(2)}, u32[]{:S(2)}) collective-permute-start(bf16[2,128,128]{2,1,0:T(8,128)(2,1)S(1)} %get-tuple-element.10), channel_id=1, source_target_pairs={{0,8},{8,16},{16,24},{1,9},{9,17},{17,25},{2,10},{10,18},{18,26},{... | collective-permute-start | bytes 196616 | tf_op jit(solution)/shard_map/ppermute | solution.py:27
  4.6 7.8 %collective-permute-start.1 = (bf16[2,128,128]{2,1,0:T(8,128)(2,1)S(1)}, bf16[2,128,128]{2,1,0:T(8,128)(2,1)S(1)}, u32[]{:S(2)}, u32[]{:S(2)}) collective-permute-start(bf16[2,128,128]{2,1,0:T(8,128)(2,1)S(1)} %get-tuple-element.11), channel_id=1, source_target_pairs={{8,0},{16,8},{24,16},{9,1},{17,9},{25,17},{10,2},{18,10},{26,18},{... | collective-permute-start | bytes 196616 | tf_op jit(solution)/shard_map/ppermute | solution.py:30
  12.9 0.7 copy-start.4
  19.2 43.9 %copy-start.1 = (bf16[128,2048]{1,0:T(8,128)(2,1)S(1)}, bf16[128,2048]{1,0:T(8,128)(2,1)}, u32[]{:S(2)}) copy-start(bf16[128,2048]{1,0:T(8,128)(2,1)} %param.19) | copy-start | bytes 1572868
  19.2 43.9 %copy-start.2 = (f32[2048]{0:T(1024)S(1)}, f32[2048]{0:T(1024)}, u32[]{:S(2)}) copy-start(f32[2048]{0:T(1024)} %param.20) | copy-start | bytes 24580
  19.2 45.5 %copy-start.3 = (f32[2048]{0:T(1024)S(1)}, f32[2048]{0:T(1024)}, u32[]{:S(2)}) copy-start(f32[2048]{0:T(1024)} %param.21) | copy-start | bytes 24580

commit v2 on v1

--- a/solution.py
+++ b/solution.py
@@ -1,5 +1,3 @@
-import functools
-
 import jax
 import jax.numpy as jnp
 from jax import lax
@@ -12,83 +10,16 @@
 HEAD_DIM = 128
 WINDOW = 128
 BLOCK = 128
-GROUP_EXPERTS = 3
 
 
 EPS = 1e-06
 NEG_BIG = -1e30
 
 
-def extended(block, sides, width):
-    for axis, dim in sides:
-        count = lax.axis_size(axis)
-        forward = [(i, i + 1) for i in range(count - 1)]
-        backward = [(target, source) for source, target in forward]
-        low = lax.ppermute(
-            lax.slice_in_dim(block, block.shape[dim] - width, None, axis=dim), axis, forward
-        )
-        high = lax.ppermute(lax.slice_in_dim(block, 0, width, axis=dim), axis, backward)
-        block = jnp.concatenate([low, block, high], axis=dim)
-    return block
-
-
-def window_attention(queries, key_heads, value_heads, sink_logit):
-    seq_rows = queries.shape[0]
-    heads_dev = sink_logit.shape[0]
-    key_group = HEADS // KV_HEADS
-    key_start = lax.axis_index("tp") * heads_dev // key_group * HEAD_DIM
-    key_own = lax.dynamic_slice_in_dim(key_heads, key_start, HEAD_DIM, 1)
-    value_own = lax.dynamic_slice_in_dim(value_heads, key_start, HEAD_DIM, 1)
-    padded = extended(jnp.stack([key_own, value_own]), (("sp", 1),), WINDOW)
-    blocks = seq_rows // BLOCK
-    extent = WINDOW // BLOCK
-    tile_rows = padded.reshape(2, blocks + 2 * extent, BLOCK, HEAD_DIM)
-    key_spans = jnp.concatenate(
-        [tile_rows[:, shifted : shifted + blocks] for shifted in range(2 * extent + 1)], axis=2
-    )
-    offset = lax.axis_index("sp") * seq_rows
-    seq_total = seq_rows * lax.axis_size("sp")
-    query_pos = offset + jnp.arange(seq_rows, dtype=jnp.int32).reshape(blocks, BLOCK)
-    key_pos = (
-        offset
-        + (jnp.arange(blocks, dtype=jnp.int32) * BLOCK)[:, None]
-        + jnp.arange(BLOCK + 2 * WINDOW, dtype=jnp.int32)[None, :]
-        - WINDOW
-    )
-    inside = (
-        (jnp.abs(query_pos[:, :, None] - key_pos[:, None, :]) <= WINDOW)
-        & (key_pos >= 0)[:, None, :]
-        & (key_pos < seq_total)[:, None, :]
-    )
-    query_blocks = queries.reshape(blocks, BLOCK, heads_dev, HEAD_DIM)
-    scores = jnp.einsum(
-        "nqhd,nkd->nhqk", query_blocks, key_spans[0], preferred_element_type=jnp.float32
-    ) * HEAD_DIM ** (-0.5)
-    scores = jnp.where(inside[:, None], scores, NEG_BIG)
-    sink_col = sink_logit[None, :, None, None]
-    row_top = jnp.maximum(jnp.max(scores, axis=3, keepdims=True), sink_col)
-    exp_terms = jnp.exp(scores - row_top)
-    row_mass = jnp.sum(exp_terms, axis=3, keepdims=True) + jnp.exp(sink_col - row_top)
-    weight = (exp_terms / row_mass).astype(jnp.bfloat16)
-    attended = jnp.einsum(
-        "nhqk,nkd->nqhd", weight, key_spans[1], preferred_element_type=jnp.float32
-    ).astype(jnp.bfloat16)
-    return attended.reshape(seq_rows, heads_dev * HEAD_DIM)
-
-
 CORES = 2
 LANES = 128
+VMEM_BYTES = 67043328
 VMEM_SPEC = pl.BlockSpec(memory_space=pltpu.VMEM)
-
-
-def places():
-    count = lax.axis_size("tp") // CORES
-    me = lax.axis_index("tp")
-    chip, core = me // CORES, lax.rem(me, CORES)
-    up = lax.rem(chip + 1, count) * CORES + core
-    down = lax.rem(chip + count - 1, count) * CORES + core
-    partner = chip * CORES + 1 - core
-    return count, chip, core, (up, down), partner
 
 
 def greet(neighbours, partner, peers):
@@ -98,122 +29,6 @@
     for peer in peers:
         pl.semaphore_signal(barrier, inc=1, device_id={"sp": peer})
     pl.semaphore_wait(barrier, 3 + len(peers))
-
-
-def column_halves(width):
-    low = (width // LANES + 1) // 2 * LANES
-    return (pl.ds(0, low), pl.ds(low, width - low)), (low, width - low)
-
-
-def gather_sum_kernel(
-    home, part_ref, out_ref, pair0, pair1, hold0, hold1, got0, got1, done,
-    core_send, core_recv, ring_send, ring_recv, swap_send, swap_recv,
-):
-    count, chip, core, neighbours, partner = places()
-    pieces = part_ref.shape[1]
-    groups = lax.axis_size("sp")
-    group = lax.axis_index("sp")
-    if home:
-        order = [lax.rem(group + j, groups) for j in range(groups)]
-        order = order[1:] + order[:1]
-        peers = order[:-1]
-    else:
-        order = list(range(pieces))
-        peers = []
-    greet(neighbours, partner, peers)
-    halves, _ = column_halves(part_ref.shape[3])
-    pair, hold, got = (pair0, pair1), (hold0, hold1), (got0, got1)
-
-    def target(side, step):
-        shift = count - 1 - step if side == 0 else 1 + step
-        return lax.rem(chip + shift, count) * CORES
-
-    def across(side, step, j):
-        return pltpu.make_async_remote_copy(
-            src_ref=part_ref.at[target(side, step) + 1 - core, order[j], :, halves[side]],
-            dst_ref=pair[side].at[step, j],
-            send_sem=core_send.at[side, step, j],
-            recv_sem=core_recv.at[side, step, j],
-            device_id={"tp": partner},
-        )
-
-    def ring(side, step, j):
-        return pltpu.make_async_remote_copy(
-            src_ref=hold[side].at[step, j],
-            dst_ref=got[side].at[step, j],
-            send_sem=ring_send.at[side, step, j],
-            recv_sem=ring_recv.at[side, step, j],
-            device_id={"tp": neighbours[side]},
-        )
-
-    def swap(j):
-        return pltpu.make_async_remote_copy(
-            src_ref=done.at[j],
-            dst_ref=out_ref.at[group],
-            send_sem=swap_send.at[j],
-            recv_sem=swap_recv.at[j],
-            device_id={"sp": order[j]},
-        )
-
-    for step in range(count):
-        for j in range(pieces):
-            for side in range(2):
-                across(side, step, j).start()
-    for step in range(count):
-        for j in range(pieces):
-            for side in range(2):
-                across(side, step, j).wait_recv()
-                value = part_ref[target(side, step) + core, order[j], :, halves[side]].astype(
-                    jnp.float32
-                ) + pair[side][step, j].astype(jnp.float32)
-                if step > 0:
-                    ring(side, step - 1, j).wait_recv()
-                    value = value + got[side][step - 1, j].astype(jnp.float32)
-                if step < count - 1:
-                    hold[side][step, j] = value.astype(hold[side].dtype)
-                    ring(side, step, j).start()
-                elif home and j < pieces - 1:
-                    done[j, :, halves[side]] = value.astype(done.dtype)
-                else:
-                    out_ref[order[j], :, halves[side]] = value.astype(out_ref.dtype)
-            if home and step == count - 1 and j < pieces - 1:
-                swap(j).start()
-    for step in range(count):
-        for j in range(pieces):
-            for side in range(2):
-                across(side, step, j).wait_send()
-                if step < count - 1:
-                    ring(side, step, j).wait_send()
-    if home:
-        for j in range(pieces - 1):
-            swap(j).wait()
-
-
-def gather_sum(part, home, out_type, collective_id):
-    total, pieces, rows, width = part.shape
-    count = total // CORES
-    _, widths = column_halves(width)
-    sem = pltpu.SemaphoreType.DMA
-    kind = part.dtype
-    return pl.pallas_call(
-        functools.partial(gather_sum_kernel, home),
-        out_shape=jax.ShapeDtypeStruct((pieces, rows, width), out_type),
-        in_specs=[VMEM_SPEC],
-        out_specs=VMEM_SPEC,
-        scratch_shapes=[
-            *[pltpu.VMEM((count, pieces, rows, w), kind) for w in widths],
-            *[pltpu.VMEM((count, pieces, rows, w), kind) for w in widths],
-            *[pltpu.VMEM((count, pieces, rows, w), kind) for w in widths],
-            pltpu.VMEM((pieces, rows, width), kind),
-            *[sem((2, count, pieces)) for _ in range(4)],
-            sem((pieces,)),
-            sem((pieces,)),
-        ],
-        compiler_params=pltpu.CompilerParams(
-            collective_id=collective_id, has_side_effects=True
-        ),
-        name="home_sum" if home else "row_sum",
-    )(part)
 
 
 def line_sequence(i, position, length, side):
@@ -522,7 +337,7 @@
     near = groups // 2
     kind = send_rows.dtype
     sem = pltpu.SemaphoreType.DMA
-    hbm = pl.BlockSpec(memory_space=pl.ANY)
+    hbm = pl.BlockSpec(memory_space=pltpu.HBM)
     total = 2 * length * groups * capacity
     return pl.pallas_call(
         moe_kernel,
@@ -553,7 +368,7 @@
             sem((groups,)),
         ],
         compiler_params=pltpu.CompilerParams(
-            collective_id=1, has_side_effects=True, vmem_limit_bytes=62 * 1024 * 1024
+            collective_id=1, has_side_effects=True, vmem_limit_bytes=VMEM_BYTES
         ),
         cost_estimate=pl.CostEstimate(
             flops=6 * total * width * members * hidden,
@@ -562,6 +377,414 @@
         ),
         name="moe",
     )(send_rows, gate_weight, up_weight, down_weight.reshape(members * hidden, width))
+
+
+def front_kernel(
+    query_hbm, key_hbm, value_hbm, sink_ref, weight_hbm, residual_hbm, mixer_hbm, expert_hbm,
+    group_ref, member_ref, gate_ref,
+    mixed_ref, rows_ref, placing_ref,
+    query, span, attended, received, full, total, residual, gains,
+    load_sem, halo_send, halo_recv, line_send, line_recv, plane_send, plane_recv,
+    core_send, core_recv, row_send, row_recv,
+):
+    parts = lax.axis_size("tp")
+    length = parts // CORES
+    tp = lax.axis_index("tp")
+    z, core = tp // CORES, lax.rem(tp, CORES)
+    partner = z * CORES + 1 - core
+    groups = lax.axis_size("sp")
+    group = lax.axis_index("sp")
+    last = length - 1
+    halves = full.shape[2]
+    relayed = groups == 4
+    seq_rows = query.shape[0]
+    heads_dev = query.shape[1] // HEAD_DIM
+    blocks = seq_rows // BLOCK
+    peers = [partner_slot(group, j, groups) for j in range(groups)]
+    sides = (
+        (lax.rem(z + length - 1, length) * CORES + core, z > 0),
+        (lax.rem(z + 1, length) * CORES + core, z < last),
+    )
+    head_start = pl.multiple_of(tp * heads_dev // (HEADS // KV_HEADS) * HEAD_DIM, HEAD_DIM)
+    inner = pl.ds(WINDOW, seq_rows)
+
+    loads = [
+        pltpu.make_async_copy(source, place, load_sem.at[n])
+        for n, (source, place) in enumerate(
+            (
+                (weight_hbm, full.at[tp]),
+                (key_hbm.at[:, pl.ds(head_start, HEAD_DIM)], span.at[0, inner]),
+                (value_hbm.at[:, pl.ds(head_start, HEAD_DIM)], span.at[1, inner]),
+                (query_hbm, query),
+                (residual_hbm, residual),
+                (mixer_hbm, gains.at[0]),
+                (expert_hbm, gains.at[1]),
+            )
+        )
+    ]
+    for copy in loads:
+        copy.start()
+
+    @pl.when(group == 0)
+    def _():
+        span[:, :WINDOW] = jnp.zeros((2, WINDOW, HEAD_DIM), span.dtype)
+
+    @pl.when(group == groups - 1)
+    def _():
+        span[:, WINDOW + seq_rows :] = jnp.zeros((2, WINDOW, HEAD_DIM), span.dtype)
+
+    barrier = pltpu.get_barrier_semaphore()
+    for shift in range(1, parts):
+        pl.semaphore_signal(barrier, inc=1, device_id={"tp": lax.rem(tp + shift, parts)})
+    for peer in peers[1:]:
+        pl.semaphore_signal(barrier, inc=1, device_id={"sp": peer})
+    pl.semaphore_wait(barrier, parts + groups - 2)
+
+    def line(side, home, half):
+        place = full.at[home * CORES + core, group, half]
+        return pltpu.make_async_remote_copy(
+            src_ref=place,
+            dst_ref=place,
+            send_sem=line_send.at[side, home, half],
+            recv_sem=line_recv.at[home, half],
+            device_id={"tp": sides[side][0]},
+        )
+
+    def plane(home, j, half, target, source):
+        place = full.at[home * CORES + core, source, half]
+        return pltpu.make_async_remote_copy(
+            src_ref=place,
+            dst_ref=place,
+            send_sem=plane_send.at[home, j, half],
+            recv_sem=plane_recv.at[home, j, half],
+            device_id={"sp": target},
+        )
+
+    def relay(home, half):
+        target, source = (peers[2], peers[1]) if half == 0 else (peers[1], peers[2])
+        return plane(home, 3, half, target, source)
+
+    def across(home):
+        place = full.at[home * CORES + core]
+        return pltpu.make_async_remote_copy(
+            src_ref=place,
+            dst_ref=place,
+            send_sem=core_send.at[home],
+            recv_sem=core_recv.at[home],
+            device_id={"tp": partner},
+        )
+
+    def halo(side):
+        start = WINDOW if side == 0 else seq_rows
+        landing = WINDOW + seq_rows if side == 0 else 0
+        return pltpu.make_async_remote_copy(
+            src_ref=span.at[:, pl.ds(start, WINDOW)],
+            dst_ref=span.at[:, pl.ds(landing, WINDOW)],
+            send_sem=halo_send.at[side],
+            recv_sem=halo_recv.at[side],
+            device_id={"sp": lax.rem(group + (groups - 1 if side == 0 else 1), groups)},
+        )
+
+    def row_block(shift):
+        target = lax.rem(tp + shift, parts)
+        return pltpu.make_async_remote_copy(
+            src_ref=attended.at[target],
+            dst_ref=received.at[tp],
+            send_sem=row_send.at[shift],
+            recv_sem=row_recv.at[shift],
+            device_id={"tp": target},
+        )
+
+    inward = (group > 0, group < groups - 1)
+    loads[0].wait()
+    for half in range(halves):
+        for side in range(2):
+            @pl.when(sides[side][1])
+            def _(side=side, half=half):
+                line(side, z, half).start()
+    loads[1].wait()
+    loads[2].wait()
+    for side in range(2):
+        @pl.when(inward[side])
+        def _(side=side):
+            halo(side).start()
+    across(z).start()
+    loads[3].wait()
+
+    def attend(n, carry):
+        b = jnp.where(n < blocks - 2, n + 1, jnp.where(n == blocks - 2, 0, blocks - 1))
+
+        @pl.when(n == blocks - 2)
+        def _():
+            for side in range(2):
+                @pl.when(inward[1 - side])
+                def _(side=side):
+                    halo(side).wait_recv()
+
+        start = pl.multiple_of(b * BLOCK, BLOCK)
+        wide = query[pl.ds(start, BLOCK), :]
+        tall = jnp.concatenate(
+            [wide[:, h * HEAD_DIM : (h + 1) * HEAD_DIM] for h in range(heads_dev)], axis=0
+        )
+        reach = BLOCK + 2 * WINDOW
+        keys = span[0, pl.ds(start, reach), :]
+        values = span[1, pl.ds(start, reach), :]
+        scores = lax.dot_general(
+            tall, keys, (((1,), (1,)), ((), ())), preferred_element_type=jnp.float32
+        ) * HEAD_DIM ** (-0.5)
+        shape = (heads_dev * BLOCK, reach)
+        row = lax.broadcasted_iota(jnp.int32, shape, 0) % BLOCK
+        column = lax.broadcasted_iota(jnp.int32, shape, 1)
+        place = column + (group * seq_rows + b * BLOCK - WINDOW)
+        inside = (
+            (column >= row) & (column <= row + 2 * WINDOW)
+            & (place >= 0) & (place < seq_rows * groups)
+        )
+        scores = jnp.where(inside, scores, NEG_BIG)
+        which = lax.broadcasted_iota(jnp.int32, (heads_dev * BLOCK, 1), 0) // BLOCK
+        sink = jnp.zeros((heads_dev * BLOCK, 1), jnp.float32)
+        for h in range(heads_dev):
+            sink = jnp.where(which == h, sink_ref[h], sink)
+        top = jnp.maximum(jnp.max(scores, axis=1, keepdims=True), sink)
+        terms = jnp.exp(scores - top)
+        mass = jnp.sum(terms, axis=1, keepdims=True) + jnp.exp(sink - top)
+        weight = (terms / mass).astype(jnp.bfloat16)
+        result = jnp.dot(weight, values, preferred_element_type=jnp.float32).astype(jnp.bfloat16)
+        attended[b] = jnp.concatenate(
+            [result[h * BLOCK : (h + 1) * BLOCK] for h in range(heads_dev)], axis=1
+        )
+        return carry
+
+    lax.fori_loop(0, blocks, attend, 0)
+    received[tp] = attended[tp]
+
+    def homes(i):
+        return ((z + 1 + i, z + 1 + i <= last), (z - 1 - i, z - 1 - i >= 0))
+
+    def spread_step(i):
+        for side in range(2):
+            home, live = homes(i)[side]
+
+            @pl.when(live)
+            def _(side=side, home=home):
+                for half in range(halves):
+                    line(side, home, half).wait_recv()
+
+                    @pl.when(sides[side][1])
+                    def _(half=half):
+                        line(side, home, half).start()
+
+                    if not relayed:
+                        for j in range(1, groups):
+                            plane(home, j, half, peers[j], group).start()
+                if relayed:
+                    for half in range(halves):
+                        plane(home, 1, half, peers[1], group).start()
+                        plane(home, 2, 1 - half, peers[2], group).start()
+
+        if relayed:
+            for side in range(2):
+                home, live = homes(i)[side]
+
+                @pl.when(live)
+                def _(home=home):
+                    for half in range(halves):
+                        plane(home, 1 + half, half, peers[1], group).wait_recv()
+                        relay(home, half).start()
+
+    spread_step(0)
+    for shift in range(1, parts):
+        row_block(shift).start()
+    for i in range(1, last):
+        spread_step(i)
+
+    slots = groups * rows_ref.shape[1]
+    tok_rows = residual.shape[0]
+    width = residual.shape[1]
+    names = lax.broadcasted_iota(jnp.int32, (groups * (8 // min(groups, 8)), tok_rows), 0)
+    chosen = (names == group_ref[...]).astype(jnp.float32)
+    earlier = (
+        lax.broadcasted_iota(jnp.int32, (tok_rows, tok_rows), 0)
+        < lax.broadcasted_iota(jnp.int32, (tok_rows, tok_rows), 1)
+    ).astype(jnp.bfloat16)
+    rank = jnp.dot(chosen.astype(jnp.bfloat16), earlier, preferred_element_type=jnp.float32)
+    slot_row = jnp.sum(
+        chosen * (rank + (names * rows_ref.shape[1]).astype(jnp.float32)), axis=0, keepdims=True
+    )
+    placing = (
+        lax.broadcasted_iota(jnp.int32, (slots, tok_rows), 0).astype(jnp.float32) == slot_row
+    ).astype(jnp.bfloat16)
+    placing_ref[...] = placing
+    members = lax.broadcasted_iota(jnp.int32, (LANES, tok_rows), 0)
+    tail = jnp.zeros((LANES, tok_rows), jnp.float32)
+    for k in range(member_ref.shape[0]):
+        tail = tail + jnp.where(
+            members == member_ref[k : k + 1, :], gate_ref[k : k + 1, :].astype(jnp.float32), 0.0
+        )
+    rows_ref[:, :, width:] = (
+        lax.dot_general(
+            placing, tail.astype(jnp.bfloat16), (((1,), (1,)), ((), ())),
+            preferred_element_type=jnp.float32,
+        )
+        .astype(rows_ref.dtype)
+        .reshape(groups, rows_ref.shape[1], LANES)
+    )
+
+    def project(home, first):
+        pieces = [received[home * CORES + c] for c in range(CORES)]
+        lhs = jnp.concatenate(pieces, axis=1)
+        rhs = jnp.concatenate(
+            [full[home * CORES + c].reshape(-1, width) for c in range(CORES)], axis=0
+        )
+        part = jnp.dot(lhs, rhs, preferred_element_type=jnp.float32)
+        if first:
+            total[...] = part
+        else:
+            total[...] += part
+
+    def rows_from(home):
+        for c in range(CORES):
+            source = home * CORES + c
+
+            @pl.when(source != tp)
+            def _(source=source):
+                shift = lax.rem(tp - source + parts, parts)
+                pltpu.make_async_remote_copy(
+                    src_ref=attended.at[source],
+                    dst_ref=received.at[source],
+                    send_sem=row_send.at[0],
+                    recv_sem=row_recv.at[lax.rem(parts + tp - source, parts)],
+                    device_id={"tp": partner},
+                ).wait_recv()
+
+    across(z).wait_recv()
+    rows_from(z)
+    project(z, True)
+
+    def gather_step(i, carry):
+        for side in range(2):
+            home, live = homes(i)[side]
+
+            @pl.when(live)
+            def _(home=home):
+                for half in range(halves):
+                    for j in range(1, groups):
+                        if not (relayed and j == 1 + half and j < 3):
+                            plane(home, j, half, peers[1], group).wait_recv()
+                across(home).start()
+
+        for side in range(2):
+            home, live = homes(i)[side]
+
+            @pl.when(live)
+            def _(home=home):
+                across(home).wait_recv()
+                rows_from(home)
+                project(home, False)
+
+        return carry
+
+    lax.fori_loop(0, last, gather_step, 0)
+
+    for copy in loads[4:]:
+        copy.wait()
+    projected = total[...]
+    scale = lax.rsqrt(jnp.mean(projected * projected, axis=1, keepdims=True) + EPS)
+    mixed = (
+        residual[...].astype(jnp.float32) + gains[0] * (projected * scale)
+    ).astype(jnp.bfloat16)
+    mixed_ref[...] = mixed
+    mixed_float = mixed.astype(jnp.float32)
+    norm = lax.rsqrt(jnp.mean(mixed_float * mixed_float, axis=1, keepdims=True) + EPS)
+    normed = (mixed_float * norm * gains[1]).astype(jnp.bfloat16)
+    rows_ref[:, :, :width] = (
+        jnp.dot(placing, normed, preferred_element_type=jnp.float32)
+        .astype(rows_ref.dtype)
+        .reshape(groups, rows_ref.shape[1], width)
+    )
+
+    for side in range(2):
+        @pl.when(inward[side])
+        def _(side=side):
+            halo(side).wait_send()
+    for shift in range(1, parts):
+        row_block(shift).wait_send()
+
+    def drain(home, carry):
+        for half in range(halves):
+            @pl.when((home >= z) & sides[0][1])
+            def _(half=half):
+                line(0, home, half).wait_send()
+
+            @pl.when((home <= z) & sides[1][1])
+            def _(half=half):
+                line(1, home, half).wait_send()
+
+            @pl.when(home != z)
+            def _(half=half):
+                for j in range(1, groups):
+                    plane(home, j, half, peers[1], group).wait_send()
+
+        across(home).wait_send()
+        return carry
+
+    lax.fori_loop(0, length, drain, 0)
+
+
+def front(
+    queries, key_heads, value_heads, sink_logit, out_weight, residual, mixer_gain, expert_gain,
+    route_group, route_member, route_weight, capacity,
+):
+    parts, groups = lax.axis_size("tp"), lax.axis_size("sp")
+    length = parts // CORES
+    seq_rows, columns = queries.shape
+    tok_rows, width = residual.shape
+    halves = 2 if groups == 4 else 1
+    piece = columns // (groups * halves)
+    sem = pltpu.SemaphoreType.DMA
+    kind = queries.dtype
+    hbm = pl.BlockSpec(memory_space=pltpu.HBM)
+    return pl.pallas_call(
+        front_kernel,
+        out_shape=(
+            jax.ShapeDtypeStruct((tok_rows, width), kind),
+            jax.ShapeDtypeStruct((groups, capacity, width + LANES), kind),
+            jax.ShapeDtypeStruct((groups * capacity, tok_rows), kind),
+        ),
+        in_specs=[hbm, hbm, hbm, pl.BlockSpec(memory_space=pltpu.SMEM), hbm, hbm, hbm, hbm,
+                  VMEM_SPEC, VMEM_SPEC, VMEM_SPEC],
+        out_specs=(VMEM_SPEC, VMEM_SPEC, VMEM_SPEC),
+        scratch_shapes=[
+            pltpu.VMEM((seq_rows, columns), kind),
+            pltpu.VMEM((2, seq_rows + 2 * WINDOW, HEAD_DIM), kind),
+            pltpu.VMEM((parts, tok_rows, columns), kind),
+            pltpu.VMEM((parts, tok_rows, columns), kind),
+            pltpu.VMEM((parts, groups, halves, piece, width), kind),
+            pltpu.VMEM((tok_rows, width), jnp.float32),
+            pltpu.VMEM((tok_rows, width), kind),
+            pltpu.VMEM((2, 1, width), jnp.float32),
+            sem((7,)),
+            sem((2,)),
+            sem((2,)),
+            sem((2, length, halves)),
+            sem((length, halves)),
+            sem((length, groups, halves)),
+            sem((length, groups, halves)),
+            sem((length,)),
+            sem((length,)),
+            sem((parts,)),
+            sem((parts,)),
+        ],
+        compiler_params=pltpu.CompilerParams(
+            collective_id=0, has_side_effects=True, vmem_limit_bytes=VMEM_BYTES
+        ),
+        name="front",
+    )(
+        queries, key_heads, value_heads, sink_logit,
+        out_weight.reshape(groups, halves, piece, width),
+        residual, mixer_gain.reshape(1, width), expert_gain.reshape(1, width),
+        route_group.reshape(1, tok_rows), route_member.T, route_weight.T,
+    )
 
 
 def per_device(
@@ -580,43 +803,13 @@
     up_weight,
     down_weight,
 ):
-    attended = window_attention(queries, key_heads, value_heads, sink_logit)
-    tok_rows = residual.shape[0]
-    width = out_weight.shape[1]
-    parts = lax.axis_size("tp")
-    pieces = 4 if tok_rows % 64 == 0 else 1
-    product = jnp.dot(attended, out_weight, preferred_element_type=jnp.float32).astype(jnp.bfloat16)
-    projected = gather_sum(
-        product.reshape(parts, pieces, tok_rows // pieces, width), False, jnp.float32, 0
-    ).reshape(tok_rows, width)
-    proj_scale = lax.rsqrt(jnp.mean(projected * projected, axis=1, keepdims=True) + EPS)
-    mixed_rows = (residual.astype(jnp.float32) + mixer_gain * (projected * proj_scale)).astype(
-        jnp.bfloat16
-    )
-    mixed_float = mixed_rows.astype(jnp.float32)
-    norm_scale = lax.rsqrt(jnp.mean(mixed_float * mixed_float, axis=1, keepdims=True) + EPS)
-    normed = (mixed_float * norm_scale * expert_gain).astype(jnp.bfloat16)
+    tok_rows, width = residual.shape
     groups = lax.axis_size("sp")
     capacity = max(2, (5 * tok_rows + 4 * groups - 1) // (4 * groups))
     capacity = (capacity + 7) // 8 * 8
-    group_ids = jnp.arange(groups, dtype=jnp.int32)
-    chosen = (route_group[:, None] == group_ids[None, :]).astype(jnp.int32)
-    group_rank = jnp.sum(chosen * (jnp.cumsum(chosen, axis=0) - 1), axis=1)
-    slot_ids = route_group * capacity + group_rank
-    placing = (jnp.arange(groups * capacity, dtype=jnp.int32)[:, None] == slot_ids[None, :]).astype(
-        jnp.bfloat16
-    )
-    member_ids = jnp.arange(GROUP_EXPERTS, dtype=jnp.int32)
-    token_gates = jnp.sum(
-        route_weight.astype(jnp.float32)[:, :, None]
-        * (route_member[:, :, None] == member_ids[None, None, :]).astype(jnp.float32),
-        axis=1,
-    ).astype(jnp.bfloat16)
-    tail = jnp.pad(token_gates, ((0, 0), (0, LANES - GROUP_EXPERTS)))
-    send_rows = (
-        jnp.dot(placing, jnp.concatenate([normed, tail], axis=1), preferred_element_type=jnp.float32)
-        .astype(jnp.bfloat16)
-        .reshape(groups, capacity, width + LANES)
+    mixed_rows, send_rows, placing = front(
+        queries, key_heads, value_heads, sink_logit, out_weight, residual, mixer_gain,
+        expert_gain, route_group, route_member, route_weight, capacity,
     )
     returned = moe(send_rows, gate_weight, up_weight, down_weight)
     expert_out = lax.dot_general(
@@ -625,7 +818,7 @@
         (((0,), (0,)), ((), ())),
         preferred_element_type=jnp.float32,
     )
-    return (mixed_float + expert_out).astype(jnp.bfloat16)
+    return (mixed_rows.astype(jnp.float32) + expert_out).astype(jnp.bfloat16)
 
 
 def solution(mesh):

time: 151 us -> 129 us (0.85)
  other arithmetic: 9.39 us -> 0 us
  matrix products: 8.35 us -> 2.37 us
  starting transfers between devices: 4.69 us -> 0 us
  local copies, waits for them, and re-layouts: 3.3 us -> 0 us
    dot_general x4 -> x0, matrix products: 6.12 us -> none  [the longest x1 3.22 us: per_device(): jnp.dot(attended, out_weight, preferred_element_type=jnp.float32)]
    ppermute x2 -> x0, starting transfers between devices: 4.69 us -> none  [the longest x1 3.4 us: extended(): lax.ppermute(lax.slice_in_dim(block, block.shape[dim] - width, None, axis...]
    reduce_sum x5 -> x0, other arithmetic: 4.58 us -> none  [the longest x1 1.61 us: per_device(): jnp.mean(mixed_float * mixed_float, axis=1, keepdims=True) + EPS]
    and x1 -> x0, other arithmetic: 1.85 us -> none  [window_attention(): (jnp.abs(query_pos[:, :, None] - key_pos[:, None, :]) <= WINDOW) & (key_p...]
    convert_element_type x3 -> x0, other arithmetic: 1.59 us -> none  [the longest x1 0.74 us: per_device(): chosen = (route_group[:, None] == group_ids[None, :]).astype(jnp.int32)]
  transfers between devices with their start and end apart: 2 -> 0, of which waited for: 0 -> 0; matrix products, arithmetic and copies ran while one was open for 4% -> 0% of each run, Pallas kernels for 0% -> 0%
where the time goes in v2:
time: 129 us; the launch traced here: 128 us
  Pallas kernels  125 us (97%)
  matrix products  2.37 us (2%)
    pallas_call x1, Pallas kernels, moe(): pl.pallas_call(moe_kernel, out_shape=jax.ShapeDtypeStruct((groups, capaci...  81.6 us
    pallas_call x1, Pallas kernels, front(): pl.pallas_call(front_kernel, out_shape=(jax.ShapeDtypeStruct((tok_rows, w...  43.7 us

profile of v2, /device:TPU:16, one launch (start us, length us, event | category | flops | bytes accessed | tf_op | source)
XLA Modules:
  0.0 127.7 jit_solution(8623023569828144560)
XLA Ops:
  0.0 43.7 %front.1 = (bf16[128,2048]{1,0:T(8,128)(2,1)}, bf16[4,40,2176]{2,1,0:T(8,128)(2,1)}, bf16[160,128]{1,0:T(8,128)(2,1)}) custom-call(bf16[1024,256]{1,0:T(8,128)(2,1)} %query_hbm.1, bf16[1024,512]{1,0:T(8,128)(2,1)} %key_hbm.1, bf16[1024,512]{1,0:T(8,128)(2,1)} %value_hbm.1, f32[2]{0:T(128)} %sink_ref.1, bf16[4,2,32,2048]{3,2,1,0:T(8,128)(2,1)} %bitcast.10, ...), custom_call_target="tpu_custom_call" | custom-call | tf_op jit(solution)/shard_map/front/pallas_call | solution.py:747
  43.7 81.6 %moe.1 = bf16[4,40,2048]{2,1,0:T(8,128)(2,1)} custom-call(bf16[4,40,2176]{2,1,0:T(8,128)(2,1)} %get-tuple-element.10.send_ref, bf16[3,2048,256]{2,1,0:T(8,128)(2,1)} %gate_hbm.1, bf16[3,2048,256]{2,1,0:T(8,128)(2,1)} %up_hbm.1, bf16[768,2048]{1,0:T(8,128)(2,1)} %bitcast.17), custom_call_target="tpu_custom_call" | custom-call | flops 12079595520 | bytes 9437184 | tf_op jit(solution)/shard_map/moe/pallas_call | solution.py:342
  125.3 2.4 %fusion = bf16[128,2048]{1,0:T(8,128)(2,1)} fusion(bf16[160,128]{1,0:T(8,128)(2,1)} %get-tuple-element.9, bf16[160,2048]{1,0:T(8,128)(2,1)} %bitcast.11, bf16[128,2048]{1,0:T(8,128)(2,1)} %get-tuple-element.8), kind=kOutput, calls=%fused_computation.1 | convolution fusion | flops 84672512 | bytes 1744896 | tf_op jit(solution)/shard_map/dot_general | solution.py:815

commit v3 on v2

--- a/solution.py
+++ b/solution.py
@@ -1,3 +1,6 @@
+import functools
+import math
+
 import jax
 import jax.numpy as jnp
 from jax import lax
@@ -19,6 +22,7 @@
 CORES = 2
 LANES = 128
 VMEM_BYTES = 67043328
+SUMMED_EIGHTHS = 3
 VMEM_SPEC = pl.BlockSpec(memory_space=pltpu.VMEM)
 
 
@@ -47,10 +51,39 @@
     return total
 
 
-def moe_kernel(
-    send_ref, gate_hbm, up_hbm, down_hbm, out_ref,
+def moe_setup(gate_hbm, up_hbm, down_hbm, inc, gate_ref, up_ref, down_ref, weight_sem):
+    length = lax.axis_size("tp") // CORES
+    z, last = lax.axis_index("tp") // CORES, length - 1
+    weights = [
+        pltpu.make_async_copy(source, place, weight_sem.at[n])
+        for n, (source, place) in enumerate(
+            ((gate_hbm, gate_ref), (up_hbm, up_ref), (down_hbm, down_ref))
+        )
+    ]
+    for copy in weights:
+        copy.start()
+
+    @pl.when((z == 0) | (z == last))
+    def _():
+        for slot in range(length):
+            @pl.when(slot != last * (z // last))
+            def _():
+                inc[slot] = jnp.zeros_like(inc[slot])
+
+        @pl.when(z == 0)
+        def _():
+            inc[0] = jnp.zeros_like(inc[0])
+
+        @pl.when(z == last)
+        def _():
+            inc[length] = jnp.zeros_like(inc[length])
+    return weights
+
+
+def moe_body(
+    weights, landed, send_ref, out_ref,
     rows, res, pair, inc, gate_ref, up_ref, down_ref,
-    weight_sem, own_sem, swap_send, swap_recv, line_send, line_recv, core_send, core_recv,
+    own_sem, swap_send, swap_recv, line_send, line_recv, core_send, core_recv,
     pair_send, pair_recv, sum_send, sum_recv, home_send, home_recv,
 ):
     length = lax.axis_size("tp") // CORES
@@ -66,33 +99,7 @@
         (lax.rem(z + length - 1, length) * CORES + core, z > 0),
         (lax.rem(z + 1, length) * CORES + core, z < last),
     )
-    peers = [partner_slot(group, j, groups) for j in range(groups)]
-
-    weights = [
-        pltpu.make_async_copy(source, place, weight_sem.at[n])
-        for n, (source, place) in enumerate(
-            ((gate_hbm, gate_ref), (up_hbm, up_ref), (down_hbm, down_ref))
-        )
-    ]
-    for copy in weights:
-        copy.start()
-
-    @pl.when((z == 0) | (z == last))
-    def _():
-        for slot in range(length):
-            @pl.when(slot != last * (z // last))
-            def _():
-                inc[slot] = jnp.zeros_like(inc[slot])
-
-        @pl.when(z == 0)
-        def _():
-            inc[0] = jnp.zeros_like(inc[0])
-
-        @pl.when(z == last)
-        def _():
-            inc[length] = jnp.zeros_like(inc[length])
-
-    greet((sides[0][0], sides[1][0]), partner, peers[1:])
+    peers = [partner_slot(group, -j % groups, groups) for j in range(groups)]
 
     def swap(j):
         return pltpu.make_async_remote_copy(
@@ -304,9 +311,13 @@
     lax.fori_loop(0, 2 * length - 1, step, 0)
     finish(1)
 
+    for j in range(groups):
+        if j > 0:
+            back(j // near, j % near).wait_recv()
+        landed(peers[j])
     for j in range(1, groups):
         swap(j).wait_send()
-        back(j // near, j % near).wait()
+        back(j // near, j % near).wait_send()
 
     def drain(index, carry):
         home = index // 2
@@ -330,62 +341,74 @@
     lax.fori_loop(0, 2 * length, drain, 0)
 
 
+def moe_kernel(send_ref, gate_hbm, up_hbm, down_hbm, out_ref, *scratch):
+    *buffers, weight_sem = scratch
+    inc, places = buffers[3], buffers[4:7]
+    weights = moe_setup(gate_hbm, up_hbm, down_hbm, inc, *places, weight_sem)
+    z, core = lax.axis_index("tp") // CORES, lax.rem(lax.axis_index("tp"), CORES)
+    length, groups = lax.axis_size("tp") // CORES, lax.axis_size("sp")
+    around = [lax.rem(z + shift, length) * CORES + core for shift in (length - 1, 1)]
+    others = [lax.rem(lax.axis_index("sp") + shift, groups) for shift in range(1, groups)]
+    greet(around, z * CORES + 1 - core, others)
+    moe_body(weights, lambda group: None, send_ref, out_ref, *buffers)
+
+
+def moe_scratch(length, groups, capacity, padded, gate_weight):
+    members, width, hidden = gate_weight.shape
+    near = groups // 2
+    kind = gate_weight.dtype
+    sem = pltpu.SemaphoreType.DMA
+    return [
+        pltpu.VMEM((2 * length, 2, near, capacity, padded), kind),
+        pltpu.VMEM((2 * length, 2, near, capacity, width), kind),
+        pltpu.VMEM((2 * length, near, capacity, width), kind),
+        pltpu.VMEM((length + 1, 2, near, capacity, width), kind),
+        pltpu.VMEM((members, width, hidden), kind),
+        pltpu.VMEM((members, width, hidden), kind),
+        pltpu.VMEM((members * hidden, width), kind),
+        sem,
+        sem((groups,)),
+        sem((groups,)),
+        sem((2, 2 * length, near)),
+        sem((2 * length, near)),
+        sem((2 * length, near)),
+        sem((2 * length, near)),
+        sem((2 * length,)),
+        sem((2 * length,)),
+        sem((2 * length, near)),
+        sem((length + 1, 2, near)),
+        sem((groups,)),
+        sem((groups,)),
+        sem((3,)),
+    ]
+
+
 def moe(send_rows, gate_weight, up_weight, down_weight):
     groups, capacity, padded = send_rows.shape
     members, width, hidden = gate_weight.shape
     length = lax.axis_size("tp") // CORES
-    near = groups // 2
-    kind = send_rows.dtype
-    sem = pltpu.SemaphoreType.DMA
     hbm = pl.BlockSpec(memory_space=pltpu.HBM)
-    total = 2 * length * groups * capacity
     return pl.pallas_call(
         moe_kernel,
-        out_shape=jax.ShapeDtypeStruct((groups, capacity, width), kind),
+        out_shape=jax.ShapeDtypeStruct((groups, capacity, width), send_rows.dtype),
         in_specs=[VMEM_SPEC, hbm, hbm, hbm],
         out_specs=VMEM_SPEC,
-        scratch_shapes=[
-            pltpu.VMEM((2 * length, 2, near, capacity, padded), kind),
-            pltpu.VMEM((2 * length, 2, near, capacity, width), kind),
-            pltpu.VMEM((2 * length, near, capacity, width), kind),
-            pltpu.VMEM((length + 1, 2, near, capacity, width), kind),
-            pltpu.VMEM((members, width, hidden), kind),
-            pltpu.VMEM((members, width, hidden), kind),
-            pltpu.VMEM((members * hidden, width), kind),
-            sem((3,)),
-            sem,
-            sem((groups,)),
-            sem((groups,)),
-            sem((2, 2 * length, near)),
-            sem((2 * length, near)),
-            sem((2 * length, near)),
-            sem((2 * length, near)),
-            sem((2 * length,)),
-            sem((2 * length,)),
-            sem((2 * length, near)),
-            sem((length + 1, 2, near)),
-            sem((groups,)),
-            sem((groups,)),
-        ],
+        scratch_shapes=moe_scratch(length, groups, capacity, padded, gate_weight),
         compiler_params=pltpu.CompilerParams(
             collective_id=1, has_side_effects=True, vmem_limit_bytes=VMEM_BYTES
         ),
-        cost_estimate=pl.CostEstimate(
-            flops=6 * total * width * members * hidden,
-            bytes_accessed=6 * members * hidden * width,
-            transcendentals=total * members * hidden,
-        ),
         name="moe",
     )(send_rows, gate_weight, up_weight, down_weight.reshape(members * hidden, width))
 
 
-def front_kernel(
-    query_hbm, key_hbm, value_hbm, sink_ref, weight_hbm, residual_hbm, mixer_hbm, expert_hbm,
+def front_body(
+    setup, query_hbm, key_hbm, value_hbm, sink_ref, weight_hbm, residual_hbm, mixer_hbm, expert_hbm,
     group_ref, member_ref, gate_ref,
     mixed_ref, rows_ref, placing_ref,
     query, span, attended, received, full, total, residual, gains,
+    own_weight, prod, prod_pair, prod_inc,
     load_sem, halo_send, halo_recv, line_send, line_recv, plane_send, plane_recv,
-    core_send, core_recv, row_send, row_recv,
+    core_send, core_recv, row_send, row_recv, pair_send, pair_recv, sum_send, sum_recv,
 ):
     parts = lax.axis_size("tp")
     length = parts // CORES
@@ -407,15 +430,17 @@
     )
     head_start = pl.multiple_of(tp * heads_dev // (HEADS // KV_HEADS) * HEAD_DIM, HEAD_DIM)
     inner = pl.ds(WINDOW, seq_rows)
+    summed, gathered = own_weight.shape[3], full.shape[4]
 
     loads = [
         pltpu.make_async_copy(source, place, load_sem.at[n])
         for n, (source, place) in enumerate(
             (
-                (weight_hbm, full.at[tp]),
+                (weight_hbm.at[:, :, :, pl.ds(summed, gathered)], full.at[tp]),
                 (key_hbm.at[:, pl.ds(head_start, HEAD_DIM)], span.at[0, inner]),
                 (value_hbm.at[:, pl.ds(head_start, HEAD_DIM)], span.at[1, inner]),
                 (query_hbm, query),
+                (weight_hbm.at[:, :, :, pl.ds(0, summed)], own_weight),
                 (residual_hbm, residual),
                 (mixer_hbm, gains.at[0]),
                 (expert_hbm, gains.at[1]),
@@ -429,10 +454,21 @@
     def _():
         span[:, :WINDOW] = jnp.zeros((2, WINDOW, HEAD_DIM), span.dtype)
 
+    @pl.when(z == 0)
+    def _():
+        for slot in range(length):
+            prod_inc[slot] = jnp.zeros_like(prod_inc[slot])
+
+    @pl.when(z == last)
+    def _():
+        for slot in [*range(last), length]:
+            prod_inc[slot] = jnp.zeros_like(prod_inc[slot])
+
     @pl.when(group == groups - 1)
     def _():
         span[:, WINDOW + seq_rows :] = jnp.zeros((2, WINDOW, HEAD_DIM), span.dtype)
 
+    started = setup()
     barrier = pltpu.get_barrier_semaphore()
     for shift in range(1, parts):
         pl.semaphore_signal(barrier, inc=1, device_id={"tp": lax.rem(tp + shift, parts)})
@@ -494,6 +530,48 @@
             recv_sem=row_recv.at[shift],
             device_id={"tp": target},
         )
+
+    def share(home):
+        return pltpu.make_async_remote_copy(
+            src_ref=prod.at[home, 1 - core],
+            dst_ref=prod_pair.at[home],
+            send_sem=pair_send.at[home],
+            recv_sem=pair_recv.at[home],
+            device_id={"tp": partner},
+        )
+
+    def add_on(side, home):
+        slot = home if side == 1 else jnp.where(home == z - 1, length, home)
+        return pltpu.make_async_remote_copy(
+            src_ref=prod.at[home, core],
+            dst_ref=prod_inc.at[slot],
+            send_sem=sum_send.at[home],
+            recv_sem=sum_recv.at[slot],
+            device_id={"tp": sides[side][0]},
+        )
+
+    def added(slot):
+        return pltpu.make_async_remote_copy(
+            src_ref=prod_inc.at[slot],
+            dst_ref=prod_inc.at[slot],
+            send_sem=sum_send.at[0],
+            recv_sem=sum_recv.at[slot],
+            device_id={"tp": partner},
+        )
+
+    def pass_on(side, home):
+        share(home).wait_recv()
+
+        @pl.when(sides[1 - side][1])
+        def _():
+            added(home).wait_recv()
+
+        prod[home, core] = (
+            prod[home, core].astype(jnp.float32)
+            + prod_pair[home].astype(jnp.float32)
+            + prod_inc[home].astype(jnp.float32)
+        ).astype(prod.dtype)
+        add_on(side, home).start()
 
     inward = (group > 0, group < groups - 1)
     loads[0].wait()
@@ -510,6 +588,7 @@
             halo(side).start()
     across(z).start()
     loads[3].wait()
+    loads[4].wait()
 
     def attend(n, carry):
         b = jnp.where(n < blocks - 2, n + 1, jnp.where(n == blocks - 2, 0, blocks - 1))
@@ -555,50 +634,90 @@
         )
         return carry
 
+
+    def homes(i):
+        return ((z + 1 + i, z + 1 + i <= last), (z - 1 - i, z - 1 - i >= 0))
+
+    def spread_half(i, half):
+        for side in range(2):
+            home, live = homes(i)[side]
+
+            @pl.when(live)
+            def _(side=side, home=home):
+                line(side, home, half).wait_recv()
+
+                @pl.when(sides[side][1])
+                def _():
+                    line(side, home, half).start()
+
+                if not relayed:
+                    for j in range(1, groups):
+                        plane(home, j, half, peers[j], group).start()
+                elif half == 0:
+                    plane(home, 1, 0, peers[1], group).start()
+                else:
+                    plane(home, 2, 1, peers[2], group).start()
+                    plane(home, 1, 1, peers[1], group).start()
+                    plane(home, 2, 0, peers[2], group).start()
+
+    def relay_half(i, half):
+        for side in range(2):
+            home, live = homes(i)[side]
+
+            @pl.when(live)
+            def _(home=home):
+                plane(home, 1 + half, half, peers[1], group).wait_recv()
+                relay(home, half).start()
+
+    def multiply(home, carry):
+        lhs = jnp.concatenate([attended[home * CORES + c] for c in range(CORES)], axis=0)
+        part = jnp.dot(
+            lhs, own_weight[...].reshape(-1, summed), preferred_element_type=jnp.float32
+        )
+        prod[home] = part.astype(prod.dtype).reshape(CORES, -1, summed)
+        share(home).start()
+        return carry
+
+    depths = (last - z, z)
+
+    def add_step(r):
+        for side in range(2):
+            event = r - (depths[side] - 1)
+            home = last - event if side == 1 else event
+
+            @pl.when((depths[side] > 0) & (event >= 0) & (event < depths[1 - side]))
+            def _(side=side, home=home):
+                pass_on(side, home)
+
+    def spread(i):
+        for half in range(halves):
+            spread_half(i, half)
+        if relayed:
+            for half in range(halves):
+                relay_half(i, half)
+
+    def first_sums():
+        for side in range(2):
+            @pl.when(depths[side] == 0)
+            def _(side=side):
+                for event in range(last):
+                    pass_on(side, last - event if side == 1 else event)
+
+    def send_rows():
+        for shift in range(1, parts):
+            row_block(shift).start()
+
     lax.fori_loop(0, blocks, attend, 0)
     received[tp] = attended[tp]
-
-    def homes(i):
-        return ((z + 1 + i, z + 1 + i <= last), (z - 1 - i, z - 1 - i >= 0))
-
-    def spread_step(i):
-        for side in range(2):
-            home, live = homes(i)[side]
-
-            @pl.when(live)
-            def _(side=side, home=home):
-                for half in range(halves):
-                    line(side, home, half).wait_recv()
-
-                    @pl.when(sides[side][1])
-                    def _(half=half):
-                        line(side, home, half).start()
-
-                    if not relayed:
-                        for j in range(1, groups):
-                            plane(home, j, half, peers[j], group).start()
-                if relayed:
-                    for half in range(halves):
-                        plane(home, 1, half, peers[1], group).start()
-                        plane(home, 2, 1 - half, peers[2], group).start()
-
-        if relayed:
-            for side in range(2):
-                home, live = homes(i)[side]
-
-                @pl.when(live)
-                def _(home=home):
-                    for half in range(halves):
-                        plane(home, 1 + half, half, peers[1], group).wait_recv()
-                        relay(home, half).start()
-
-    spread_step(0)
-    for shift in range(1, parts):
-        row_block(shift).start()
+    send_rows()
+    lax.fori_loop(0, length, multiply, 0)
+    spread(0)
+    first_sums()
     for i in range(1, last):
-        spread_step(i)
-
-    slots = groups * rows_ref.shape[1]
+        add_step(i - 1)
+        spread(i)
+    capacity = rows_ref.shape[1]
+    slots = groups * capacity
     tok_rows = residual.shape[0]
     width = residual.shape[1]
     names = lax.broadcasted_iota(jnp.int32, (groups * (8 // min(groups, 8)), tok_rows), 0)
@@ -614,7 +733,7 @@
     placing = (
         lax.broadcasted_iota(jnp.int32, (slots, tok_rows), 0).astype(jnp.float32) == slot_row
     ).astype(jnp.bfloat16)
-    placing_ref[...] = placing
+    placing_ref[...] = placing.reshape(placing_ref.shape)
     members = lax.broadcasted_iota(jnp.int32, (LANES, tok_rows), 0)
     tail = jnp.zeros((LANES, tok_rows), jnp.float32)
     for k in range(member_ref.shape[0]):
@@ -634,13 +753,13 @@
         pieces = [received[home * CORES + c] for c in range(CORES)]
         lhs = jnp.concatenate(pieces, axis=1)
         rhs = jnp.concatenate(
-            [full[home * CORES + c].reshape(-1, width) for c in range(CORES)], axis=0
+            [full[home * CORES + c].reshape(-1, gathered) for c in range(CORES)], axis=0
         )
         part = jnp.dot(lhs, rhs, preferred_element_type=jnp.float32)
         if first:
-            total[...] = part
+            total[:, summed:] = part
         else:
-            total[...] += part
+            total[:, summed:] += part
 
     def rows_from(home):
         for c in range(CORES):
@@ -686,7 +805,23 @@
 
     lax.fori_loop(0, last, gather_step, 0)
 
-    for copy in loads[4:]:
+    share(z).wait_recv()
+
+    @pl.when(z > 0)
+    def _():
+        added(z).wait_recv()
+
+    @pl.when(z < last)
+    def _():
+        added(length).wait_recv()
+
+    total[:, :summed] = (
+        prod[z, core].astype(jnp.float32)
+        + prod_pair[z].astype(jnp.float32)
+        + prod_inc[z].astype(jnp.float32)
+        + prod_inc[length].astype(jnp.float32)
+    )
+    for copy in loads[5:]:
         copy.wait()
     projected = total[...]
     scale = lax.rsqrt(jnp.mean(projected * projected, axis=1, keepdims=True) + EPS)
@@ -703,88 +838,163 @@
         .reshape(groups, rows_ref.shape[1], width)
     )
 
-    for side in range(2):
-        @pl.when(inward[side])
-        def _(side=side):
-            halo(side).wait_send()
-    for shift in range(1, parts):
-        row_block(shift).wait_send()
-
-    def drain(home, carry):
-        for half in range(halves):
-            @pl.when((home >= z) & sides[0][1])
-            def _(half=half):
-                line(0, home, half).wait_send()
-
-            @pl.when((home <= z) & sides[1][1])
-            def _(half=half):
-                line(1, home, half).wait_send()
+    def settle():
+        for side in range(2):
+            @pl.when(inward[side])
+            def _(side=side):
+                halo(side).wait_send()
+        for shift in range(1, parts):
+            row_block(shift).wait_send()
+
+        def drain(home, carry):
+            for half in range(halves):
+                @pl.when((home >= z) & sides[0][1])
+                def _(half=half):
+                    line(0, home, half).wait_send()
+
+                @pl.when((home <= z) & sides[1][1])
+                def _(half=half):
+                    line(1, home, half).wait_send()
+
+                @pl.when(home != z)
+                def _(half=half):
+                    for j in range(1, groups):
+                        plane(home, j, half, peers[1], group).wait_send()
 
             @pl.when(home != z)
-            def _(half=half):
-                for j in range(1, groups):
-                    plane(home, j, half, peers[1], group).wait_send()
-
-        across(home).wait_send()
-        return carry
-
-    lax.fori_loop(0, length, drain, 0)
-
-
-def front(
-    queries, key_heads, value_heads, sink_logit, out_weight, residual, mixer_gain, expert_gain,
-    route_group, route_member, route_weight, capacity,
-):
-    parts, groups = lax.axis_size("tp"), lax.axis_size("sp")
+            def _():
+                add_on(1, home).wait_send()
+
+            across(home).wait_send()
+            share(home).wait_send()
+            return carry
+
+        lax.fori_loop(0, length, drain, 0)
+
+    return started, settle
+
+
+def front_kernel(*refs):
+    _, settle = front_body(lambda: None, *refs)
+    settle()
+
+
+def front_scratch(parts, groups, queries, residual):
     length = parts // CORES
     seq_rows, columns = queries.shape
     tok_rows, width = residual.shape
     halves = 2 if groups == 4 else 1
     piece = columns // (groups * halves)
+    summed = SUMMED_EIGHTHS * width // 8 // LANES * LANES
     sem = pltpu.SemaphoreType.DMA
     kind = queries.dtype
-    hbm = pl.BlockSpec(memory_space=pltpu.HBM)
+    return [
+        pltpu.VMEM((seq_rows, columns), kind),
+        pltpu.VMEM((2, seq_rows + 2 * WINDOW, HEAD_DIM), kind),
+        pltpu.VMEM((parts, tok_rows, columns), kind),
+        pltpu.VMEM((parts, tok_rows, columns), kind),
+        pltpu.VMEM((parts, groups, halves, piece, width - summed), kind),
+        pltpu.VMEM((tok_rows, width), jnp.float32),
+        pltpu.VMEM((tok_rows, width), kind),
+        pltpu.VMEM((2, 1, width), jnp.float32),
+        pltpu.VMEM((groups, halves, piece, summed), kind),
+        pltpu.VMEM((length, CORES, tok_rows, summed), kind),
+        pltpu.VMEM((length, tok_rows, summed), kind),
+        pltpu.VMEM((length + 1, tok_rows, summed), kind),
+        sem((8,)),
+        sem((2,)),
+        sem((2,)),
+        sem((2, length, halves)),
+        sem((length, halves)),
+        sem((length, groups, halves)),
+        sem((length, groups, halves)),
+        sem((length,)),
+        sem((length,)),
+        sem((parts,)),
+        sem((parts,)),
+        sem((length,)),
+        sem((length,)),
+        sem((length,)),
+        sem((length + 1,)),
+    ]
+
+
+HBM_SPEC = pl.BlockSpec(memory_space=pltpu.HBM)
+FRONT_SPECS = (
+    *[HBM_SPEC] * 3, pl.BlockSpec(memory_space=pltpu.SMEM), *[HBM_SPEC] * 4, *[VMEM_SPEC] * 3
+)
+
+
+def front_made(groups, capacity, residual):
+    tok_rows, width = residual.shape
+    return (
+        ((tok_rows, width), residual.dtype),
+        ((groups, capacity, width + LANES), residual.dtype),
+        ((groups, capacity, tok_rows), residual.dtype),
+    )
+
+
+def front(arguments, capacity):
+    parts, groups = lax.axis_size("tp"), lax.axis_size("sp")
+    made = front_made(groups, capacity, arguments[5])
     return pl.pallas_call(
         front_kernel,
-        out_shape=(
-            jax.ShapeDtypeStruct((tok_rows, width), kind),
-            jax.ShapeDtypeStruct((groups, capacity, width + LANES), kind),
-            jax.ShapeDtypeStruct((groups * capacity, tok_rows), kind),
-        ),
-        in_specs=[hbm, hbm, hbm, pl.BlockSpec(memory_space=pltpu.SMEM), hbm, hbm, hbm, hbm,
-                  VMEM_SPEC, VMEM_SPEC, VMEM_SPEC],
-        out_specs=(VMEM_SPEC, VMEM_SPEC, VMEM_SPEC),
-        scratch_shapes=[
-            pltpu.VMEM((seq_rows, columns), kind),
-            pltpu.VMEM((2, seq_rows + 2 * WINDOW, HEAD_DIM), kind),
-            pltpu.VMEM((parts, tok_rows, columns), kind),
-            pltpu.VMEM((parts, tok_rows, columns), kind),
-            pltpu.VMEM((parts, groups, halves, piece, width), kind),
-            pltpu.VMEM((tok_rows, width), jnp.float32),
-            pltpu.VMEM((tok_rows, width), kind),
-            pltpu.VMEM((2, 1, width), jnp.float32),
-            sem((7,)),
-            sem((2,)),
-            sem((2,)),
-            sem((2, length, halves)),
-            sem((length, halves)),
-            sem((length, groups, halves)),
-            sem((length, groups, halves)),
-            sem((length,)),
-            sem((length,)),
-            sem((parts,)),
-            sem((parts,)),
-        ],
+        out_shape=[jax.ShapeDtypeStruct(*each) for each in made],
+        in_specs=FRONT_SPECS,
+        out_specs=[VMEM_SPEC] * 3,
+        scratch_shapes=front_scratch(parts, groups, arguments[0], arguments[5]),
         compiler_params=pltpu.CompilerParams(
             collective_id=0, has_side_effects=True, vmem_limit_bytes=VMEM_BYTES
         ),
         name="front",
-    )(
-        queries, key_heads, value_heads, sink_logit,
-        out_weight.reshape(groups, halves, piece, width),
-        residual, mixer_gain.reshape(1, width), expert_gain.reshape(1, width),
-        route_group.reshape(1, tok_rows), route_member.T, route_weight.T,
-    )
+    )(*arguments)
+
+
+def layer_kernel(inputs, front_count, moe_count, *refs):
+    front_in, refs = refs[:inputs], refs[inputs:]
+    weights_in, out_ref, refs = refs[:3], refs[3], refs[4:]
+    front_refs, refs = refs[:front_count], refs[front_count:]
+    *buffers, weight_sem = refs[:moe_count]
+    mixed_ref, rows_ref, placing_ref, returned = refs[moe_count:]
+
+    def setup():
+        return moe_setup(*weights_in, buffers[3], *buffers[4:7], weight_sem)
+
+    weights, settle = front_body(
+        setup, *front_in, mixed_ref, rows_ref, placing_ref, *front_refs
+    )
+    total = front_refs[5]
+    total[...] = mixed_ref[...].astype(jnp.float32)
+
+    def landed(group):
+        total[...] += lax.dot_general(
+            placing_ref[group], returned[group], (((0,), (0,)), ((), ())),
+            preferred_element_type=jnp.float32,
+        )
+
+    moe_body(weights, landed, rows_ref, returned, *buffers)
+    out_ref[...] = total[...].astype(out_ref.dtype)
+    settle()
+
+
+def layer(arguments, capacity, gate_weight, up_weight, down_weight, front_bufs, moe_bufs):
+    residual = arguments[5]
+    groups = lax.axis_size("sp")
+    kept = front_made(groups, capacity, residual)
+    returned = ((groups, capacity, residual.shape[1]), residual.dtype)
+    return pl.pallas_call(
+        functools.partial(layer_kernel, len(arguments), len(front_bufs), len(moe_bufs)),
+        out_shape=jax.ShapeDtypeStruct(residual.shape, residual.dtype),
+        in_specs=[*FRONT_SPECS, *[HBM_SPEC] * 3],
+        out_specs=VMEM_SPEC,
+        scratch_shapes=[
+            *front_bufs, *moe_bufs, *[pltpu.VMEM(*each) for each in (*kept, returned)]
+        ],
+        compiler_params=pltpu.CompilerParams(
+            collective_id=2, has_side_effects=True, vmem_limit_bytes=VMEM_BYTES
+        ),
+        name="layer",
+    )(*arguments, gate_weight, up_weight, down_weight.reshape(-1, residual.shape[1]))
 
 
 def per_device(
@@ -804,17 +1014,32 @@
     down_weight,
 ):
     tok_rows, width = residual.shape
-    groups = lax.axis_size("sp")
+    parts, groups = lax.axis_size("tp"), lax.axis_size("sp")
     capacity = max(2, (5 * tok_rows + 4 * groups - 1) // (4 * groups))
     capacity = (capacity + 7) // 8 * 8
-    mixed_rows, send_rows, placing = front(
-        queries, key_heads, value_heads, sink_logit, out_weight, residual, mixer_gain,
-        expert_gain, route_group, route_member, route_weight, capacity,
-    )
+    halves = 2 if groups == 4 else 1
+    arguments = (
+        queries, key_heads, value_heads, sink_logit,
+        out_weight.reshape(groups, halves, -1, width), residual,
+        mixer_gain.reshape(1, width), expert_gain.reshape(1, width),
+        route_group.reshape(1, tok_rows), route_member.T, route_weight.T,
+    )
+    front_bufs = front_scratch(parts, groups, queries, residual)
+    moe_bufs = moe_scratch(parts // CORES, groups, capacity, width + LANES, gate_weight)
+    held = sum(
+        math.prod(each.shape) * jnp.dtype(each.dtype).itemsize
+        for each in (*front_bufs, *moe_bufs)
+        if getattr(each, "memory_space", None) == pltpu.VMEM
+    )
+    if held < VMEM_BYTES * 3 // 4:
+        return layer(
+            arguments, capacity, gate_weight, up_weight, down_weight, front_bufs, moe_bufs
+        )
+    mixed_rows, send_rows, placing = front(arguments, capacity)
     returned = moe(send_rows, gate_weight, up_weight, down_weight)
     expert_out = lax.dot_general(
-        placing,
-        returned.reshape(groups * capacity, width),
+        placing.reshape(-1, tok_rows),
+        returned.reshape(-1, width),
         (((0,), (0,)), ((), ())),
         preferred_element_type=jnp.float32,
     )

time: 129 us -> 118 us (0.915)
  Pallas kernels: 125 us -> 114 us
  matrix products: 2.37 us -> 0 us
  local copies, waits for them, and re-layouts: 0 us -> 1.88 us
    pallas_call x2 -> x1, Pallas kernels: 125 us -> 114 us  [layer(): pl.pallas_call(functools.partial(layer_kernel, len(arguments), len(front_...]
    dot_general x1 -> x0, matrix products: 2.37 us -> none  [per_device(): lax.dot_general(placing, returned.reshape(groups * capacity, width), (((0...]
    unnamed x0 -> x1, local copies, waits for them, and re-layouts: none -> 1.88 us
where the time goes in v3:
time: 118 us; the launch traced here: 116 us
  Pallas kernels  114 us (97%)
  local copies, waits for them, and re-layouts  1.88 us (2%)
    pallas_call x1, Pallas kernels, layer(): pl.pallas_call(functools.partial(layer_kernel, len(arguments), len(front_...  114 us

profile of v3, /device:TPU:16, one launch (start us, length us, event | category | flops | bytes accessed | tf_op | source)
XLA Modules:
  0.0 115.8 jit_solution(10003629013042244573)
XLA Ops:
  0.0 113.9 %layer.1 = bf16[128,2048]{1,0:T(8,128)(2,1)} custom-call(bf16[1024,256]{1,0:T(8,128)(2,1)} %refs_0_.1, bf16[1024,512]{1,0:T(8,128)(2,1)} %refs_1_.1, bf16[1024,512]{1,0:T(8,128)(2,1)} %refs_2_.1, f32[2]{0:T(128)} %refs_3_.1, bf16[4,2,32,2048]{3,2,1,0:T(8,128)(2,1)} %bitcast.8, bf16[128,2048]{1,0:T(8,128)(2,1)} %refs_5_.1, f32[1,2048]{1,0:T(1,128)} %bitcast.9, ...), custom_call_target="tpu_custom_call" | custom-call | tf_op jit(solution)/shard_map/layer/pallas_call | solution.py:985
  113.9 1.9 %copy.16 = bf16[128,2048]{1,0:T(8,128)(2,1)} copy(bf16[128,2048]{1,0:T(8,128)(2,1)} %layer.1) | data formatting | bytes 1048576

commit v4 on v3

--- a/solution.py
+++ b/solution.py
@@ -23,6 +23,7 @@
 LANES = 128
 VMEM_BYTES = 67043328
 SUMMED_EIGHTHS = 3
+GATE_ROWS = 8
 VMEM_SPEC = pl.BlockSpec(memory_space=pltpu.VMEM)
 
 
@@ -81,7 +82,7 @@
 
 
 def moe_body(
-    weights, landed, send_ref, out_ref,
+    weights, landed, send_ref, gates_ref, out_ref,
     rows, res, pair, inc, gate_ref, up_ref, down_ref,
     own_sem, swap_send, swap_recv, line_send, line_recv, core_send, core_recv,
     pair_send, pair_recv, sum_send, sum_recv, home_send, home_recv,
@@ -202,12 +203,18 @@
         for j in range(near):
             across(index, j).wait_recv()
         block = rows[index].reshape(2 * near * rows.shape[3], rows.shape[4])
-        values = block[:, :width]
-        gates = block[:, width:].astype(jnp.float32)
+        home, half = index // 2, lax.rem(index, 2)
+        gates = jnp.concatenate(
+            [
+                gates_ref[home * CORES + c, half * near + j].astype(jnp.float32).T[: rows.shape[3]]
+                for c in range(CORES) for j in range(near)
+            ],
+            axis=0,
+        )
         hidden = []
         for member in range(gate_ref.shape[0]):
-            gate_pre = jnp.dot(values, gate_ref[member], preferred_element_type=jnp.float32)
-            up_pre = jnp.dot(values, up_ref[member], preferred_element_type=jnp.float32)
+            gate_pre = jnp.dot(block, gate_ref[member], preferred_element_type=jnp.float32)
+            up_pre = jnp.dot(block, up_ref[member], preferred_element_type=jnp.float32)
             value = gate_pre / (1.0 + jnp.exp(-gate_pre)) * up_pre * gates[:, member : member + 1]
             hidden.append(value.astype(jnp.bfloat16))
         total = jnp.dot(
@@ -258,6 +265,8 @@
     reaches = (last - z, z)
     lags = tuple(jnp.where(depth == 0, 0, 2 * depth + 1) for depth in (last - z, z))
 
+    spare = max(0, 2 * last - 3)
+
     def step(k, carry):
         for j in range(near):
             for side in range(2):
@@ -283,11 +292,11 @@
             home0, half0 = line_sequence(k, z, length, 0)
             home1, half1 = line_sequence(k, z, length, 1)
             index = jnp.where(
-                d == 0, home0 * 2 + half0, jnp.where(d == 1, home1 * 2 + half1, z * 2 + k // 2)
+                d == 0, home0 * 2 + half0, jnp.where(d == 1, home1 * 2 + half1, z * 2 + k - spare)
             )
             live = jnp.where(
                 d == 0, k < 2 * reaches[0],
-                jnp.where(d == 1, k < 2 * reaches[1], (k == 0) | (k == 2)),
+                jnp.where(d == 1, k < 2 * reaches[1], (k == spare) | (k == spare + 1)),
             )
 
             @pl.when(live)
@@ -314,7 +323,7 @@
     for j in range(groups):
         if j > 0:
             back(j // near, j % near).wait_recv()
-        landed(peers[j])
+        landed(j, peers[j])
     for j in range(1, groups):
         swap(j).wait_send()
         back(j // near, j % near).wait_send()
@@ -341,7 +350,7 @@
     lax.fori_loop(0, 2 * length, drain, 0)
 
 
-def moe_kernel(send_ref, gate_hbm, up_hbm, down_hbm, out_ref, *scratch):
+def moe_kernel(send_ref, gates_ref, gate_hbm, up_hbm, down_hbm, out_ref, *scratch):
     *buffers, weight_sem = scratch
     inc, places = buffers[3], buffers[4:7]
     weights = moe_setup(gate_hbm, up_hbm, down_hbm, inc, *places, weight_sem)
@@ -350,16 +359,16 @@
     around = [lax.rem(z + shift, length) * CORES + core for shift in (length - 1, 1)]
     others = [lax.rem(lax.axis_index("sp") + shift, groups) for shift in range(1, groups)]
     greet(around, z * CORES + 1 - core, others)
-    moe_body(weights, lambda group: None, send_ref, out_ref, *buffers)
-
-
-def moe_scratch(length, groups, capacity, padded, gate_weight):
+    moe_body(weights, lambda j, group: None, send_ref, gates_ref, out_ref, *buffers)
+
+
+def moe_scratch(length, groups, capacity, gate_weight):
     members, width, hidden = gate_weight.shape
     near = groups // 2
     kind = gate_weight.dtype
     sem = pltpu.SemaphoreType.DMA
     return [
-        pltpu.VMEM((2 * length, 2, near, capacity, padded), kind),
+        pltpu.VMEM((2 * length, 2, near, capacity, width), kind),
         pltpu.VMEM((2 * length, 2, near, capacity, width), kind),
         pltpu.VMEM((2 * length, near, capacity, width), kind),
         pltpu.VMEM((length + 1, 2, near, capacity, width), kind),
@@ -383,32 +392,33 @@
     ]
 
 
-def moe(send_rows, gate_weight, up_weight, down_weight):
-    groups, capacity, padded = send_rows.shape
+def moe(send_rows, gates, gate_weight, up_weight, down_weight):
+    groups, capacity, _ = send_rows.shape
     members, width, hidden = gate_weight.shape
     length = lax.axis_size("tp") // CORES
     hbm = pl.BlockSpec(memory_space=pltpu.HBM)
     return pl.pallas_call(
         moe_kernel,
         out_shape=jax.ShapeDtypeStruct((groups, capacity, width), send_rows.dtype),
-        in_specs=[VMEM_SPEC, hbm, hbm, hbm],
+        in_specs=[VMEM_SPEC, VMEM_SPEC, hbm, hbm, hbm],
         out_specs=VMEM_SPEC,
-        scratch_shapes=moe_scratch(length, groups, capacity, padded, gate_weight),
+        scratch_shapes=moe_scratch(length, groups, capacity, gate_weight),
         compiler_params=pltpu.CompilerParams(
             collective_id=1, has_side_effects=True, vmem_limit_bytes=VMEM_BYTES
         ),
         name="moe",
-    )(send_rows, gate_weight, up_weight, down_weight.reshape(members * hidden, width))
+    )(send_rows, gates, gate_weight, up_weight, down_weight.reshape(members * hidden, width))
 
 
 def front_body(
     setup, query_hbm, key_hbm, value_hbm, sink_ref, weight_hbm, residual_hbm, mixer_hbm, expert_hbm,
     group_ref, member_ref, gate_ref,
-    mixed_ref, rows_ref, placing_ref,
+    mixed_ref, rows_ref, placing_ref, gates_ref,
     query, span, attended, received, full, total, residual, gains,
-    own_weight, prod, prod_pair, prod_inc,
+    own_weight, prod, prod_pair, prod_inc, gate_rows,
     load_sem, halo_send, halo_recv, line_send, line_recv, plane_send, plane_recv,
     core_send, core_recv, row_send, row_recv, pair_send, pair_recv, sum_send, sum_recv,
+    gate_send, gate_recv, gates_send, gates_recv,
 ):
     parts = lax.axis_size("tp")
     length = parts // CORES
@@ -510,6 +520,16 @@
             device_id={"tp": partner},
         )
 
+    def across_part(home, part, half):
+        place = full.at[home * CORES + core, part, half]
+        return pltpu.make_async_remote_copy(
+            src_ref=place,
+            dst_ref=place,
+            send_sem=core_send.at[home],
+            recv_sem=core_recv.at[home],
+            device_id={"tp": partner},
+        )
+
     def halo(side):
         start = WINDOW if side == 0 else seq_rows
         landing = WINDOW + seq_rows if side == 0 else 0
@@ -572,6 +592,27 @@
             + prod_inc[home].astype(jnp.float32)
         ).astype(prod.dtype)
         add_on(side, home).start()
+
+    mirrored = [partner_slot(group, -j % groups, groups) for j in range(groups)]
+
+    def gate_swap(j):
+        return pltpu.make_async_remote_copy(
+            src_ref=gate_rows.at[mirrored[j]],
+            dst_ref=gates_ref.at[tp, j],
+            send_sem=gate_send.at[j],
+            recv_sem=gate_recv.at[j],
+            device_id={"sp": mirrored[j]},
+        )
+
+    def gate_block(shift):
+        place = gates_ref.at[tp]
+        return pltpu.make_async_remote_copy(
+            src_ref=place,
+            dst_ref=place,
+            send_sem=gates_send.at[shift],
+            recv_sem=gates_recv.at[shift],
+            device_id={"tp": lax.rem(tp + shift, parts)},
+        )
 
     inward = (group > 0, group < groups - 1)
     loads[0].wait()
@@ -650,6 +691,7 @@
                 def _():
                     line(side, home, half).start()
 
+                across_part(home, group, half).start()
                 if not relayed:
                     for j in range(1, groups):
                         plane(home, j, half, peers[j], group).start()
@@ -668,6 +710,7 @@
             def _(home=home):
                 plane(home, 1 + half, half, peers[1], group).wait_recv()
                 relay(home, half).start()
+                across_part(home, peers[1 + half], half).start()
 
     def multiply(home, carry):
         lhs = jnp.concatenate([attended[home * CORES + c] for c in range(CORES)], axis=0)
@@ -713,9 +756,6 @@
     lax.fori_loop(0, length, multiply, 0)
     spread(0)
     first_sums()
-    for i in range(1, last):
-        add_step(i - 1)
-        spread(i)
     capacity = rows_ref.shape[1]
     slots = groups * capacity
     tok_rows = residual.shape[0]
@@ -728,26 +768,31 @@
     ).astype(jnp.bfloat16)
     rank = jnp.dot(chosen.astype(jnp.bfloat16), earlier, preferred_element_type=jnp.float32)
     slot_row = jnp.sum(
-        chosen * (rank + (names * rows_ref.shape[1]).astype(jnp.float32)), axis=0, keepdims=True
+        chosen * (rank + (names * capacity).astype(jnp.float32)), axis=0, keepdims=True
     )
     placing = (
         lax.broadcasted_iota(jnp.int32, (slots, tok_rows), 0).astype(jnp.float32) == slot_row
     ).astype(jnp.bfloat16)
     placing_ref[...] = placing.reshape(placing_ref.shape)
-    members = lax.broadcasted_iota(jnp.int32, (LANES, tok_rows), 0)
-    tail = jnp.zeros((LANES, tok_rows), jnp.float32)
+    members = lax.broadcasted_iota(jnp.int32, (GATE_ROWS, tok_rows), 0)
+    tail = jnp.zeros((GATE_ROWS, tok_rows), jnp.float32)
     for k in range(member_ref.shape[0]):
         tail = tail + jnp.where(
             members == member_ref[k : k + 1, :], gate_ref[k : k + 1, :].astype(jnp.float32), 0.0
         )
-    rows_ref[:, :, width:] = (
-        lax.dot_general(
-            placing, tail.astype(jnp.bfloat16), (((1,), (1,)), ((), ())),
-            preferred_element_type=jnp.float32,
-        )
-        .astype(rows_ref.dtype)
-        .reshape(groups, rows_ref.shape[1], LANES)
-    )
+    place = lax.broadcasted_iota(jnp.int32, (LANES, tok_rows), 0)
+    for g in range(groups):
+        chosen_slot = jnp.where(place < capacity, place + g * capacity, slots).astype(jnp.float32)
+        gate_rows[g] = lax.dot_general(
+            tail.astype(jnp.bfloat16), (chosen_slot == slot_row).astype(jnp.bfloat16),
+            (((1,), (1,)), ((), ())), preferred_element_type=jnp.float32,
+        ).astype(gate_rows.dtype)
+    gates_ref[tp, 0] = gate_rows[group]
+    for j in range(1, groups):
+        gate_swap(j).start()
+    for i in range(1, last):
+        add_step(i - 1)
+        spread(i)
 
     def project(home, first):
         pieces = [received[home * CORES + c] for c in range(CORES)]
@@ -776,6 +821,10 @@
                     device_id={"tp": partner},
                 ).wait_recv()
 
+    for j in range(1, groups):
+        gate_swap(j).wait_recv()
+    for shift in range(1, parts):
+        gate_block(shift).start()
     across(z).wait_recv()
     rows_from(z)
     project(z, True)
@@ -790,7 +839,7 @@
                     for j in range(1, groups):
                         if not (relayed and j == 1 + half and j < 3):
                             plane(home, j, half, peers[1], group).wait_recv()
-                across(home).start()
+                            across_part(home, peers[j], half).start()
 
         for side in range(2):
             home, live = homes(i)[side]
@@ -832,11 +881,14 @@
     mixed_float = mixed.astype(jnp.float32)
     norm = lax.rsqrt(jnp.mean(mixed_float * mixed_float, axis=1, keepdims=True) + EPS)
     normed = (mixed_float * norm * gains[1]).astype(jnp.bfloat16)
-    rows_ref[:, :, :width] = (
+    rows_ref[...] = (
         jnp.dot(placing, normed, preferred_element_type=jnp.float32)
         .astype(rows_ref.dtype)
-        .reshape(groups, rows_ref.shape[1], width)
+        .reshape(rows_ref.shape)
     )
+
+    for shift in range(1, parts):
+        gate_block(shift).wait_recv()
 
     def settle():
         for side in range(2):
@@ -845,6 +897,9 @@
                 halo(side).wait_send()
         for shift in range(1, parts):
             row_block(shift).wait_send()
+            gate_block(shift).wait_send()
+        for j in range(1, groups):
+            gate_swap(j).wait_send()
 
         def drain(home, carry):
             for half in range(halves):
@@ -901,6 +956,7 @@
         pltpu.VMEM((length, CORES, tok_rows, summed), kind),
         pltpu.VMEM((length, tok_rows, summed), kind),
         pltpu.VMEM((length + 1, tok_rows, summed), kind),
+        pltpu.VMEM((groups, GATE_ROWS, LANES), kind),
         sem((8,)),
         sem((2,)),
         sem((2,)),
@@ -916,6 +972,10 @@
         sem((length,)),
         sem((length,)),
         sem((length + 1,)),
+        sem((groups,)),
+        sem((groups,)),
+        sem((parts,)),
+        sem((parts,)),
     ]
 
 
@@ -929,8 +989,9 @@
     tok_rows, width = residual.shape
     return (
         ((tok_rows, width), residual.dtype),
-        ((groups, capacity, width + LANES), residual.dtype),
+        ((groups, capacity, width), residual.dtype),
         ((groups, capacity, tok_rows), residual.dtype),
+        ((lax.axis_size("tp"), groups, GATE_ROWS, LANES), residual.dtype),
     )
 
 
@@ -941,7 +1002,7 @@
         front_kernel,
         out_shape=[jax.ShapeDtypeStruct(*each) for each in made],
         in_specs=FRONT_SPECS,
-        out_specs=[VMEM_SPEC] * 3,
+        out_specs=[VMEM_SPEC] * 4,
         scratch_shapes=front_scratch(parts, groups, arguments[0], arguments[5]),
         compiler_params=pltpu.CompilerParams(
             collective_id=0, has_side_effects=True, vmem_limit_bytes=VMEM_BYTES
@@ -955,24 +1016,24 @@
     weights_in, out_ref, refs = refs[:3], refs[3], refs[4:]
     front_refs, refs = refs[:front_count], refs[front_count:]
     *buffers, weight_sem = refs[:moe_count]
-    mixed_ref, rows_ref, placing_ref, returned = refs[moe_count:]
+    mixed_ref, rows_ref, placing_ref, gates_ref, returned = refs[moe_count:]
 
     def setup():
         return moe_setup(*weights_in, buffers[3], *buffers[4:7], weight_sem)
 
     weights, settle = front_body(
-        setup, *front_in, mixed_ref, rows_ref, placing_ref, *front_refs
+        setup, *front_in, mixed_ref, rows_ref, placing_ref, gates_ref, *front_refs
     )
     total = front_refs[5]
-    total[...] = mixed_ref[...].astype(jnp.float32)
-
-    def landed(group):
-        total[...] += lax.dot_general(
+
+    def landed(j, group):
+        part = lax.dot_general(
             placing_ref[group], returned[group], (((0,), (0,)), ((), ())),
             preferred_element_type=jnp.float32,
         )
-
-    moe_body(weights, landed, rows_ref, returned, *buffers)
+        total[...] = (mixed_ref[...].astype(jnp.float32) if j == 0 else total[...]) + part
+
+    moe_body(weights, landed, rows_ref, gates_ref, returned, *buffers)
     out_ref[...] = total[...].astype(out_ref.dtype)
     settle()
 
@@ -1025,7 +1086,7 @@
         route_group.reshape(1, tok_rows), route_member.T, route_weight.T,
     )
     front_bufs = front_scratch(parts, groups, queries, residual)
-    moe_bufs = moe_scratch(parts // CORES, groups, capacity, width + LANES, gate_weight)
+    moe_bufs = moe_scratch(parts // CORES, groups, capacity, gate_weight)
     held = sum(
         math.prod(each.shape) * jnp.dtype(each.dtype).itemsize
         for each in (*front_bufs, *moe_bufs)
@@ -1035,8 +1096,8 @@
         return layer(
             arguments, capacity, gate_weight, up_weight, down_weight, front_bufs, moe_bufs
         )
-    mixed_rows, send_rows, placing = front(arguments, capacity)
-    returned = moe(send_rows, gate_weight, up_weight, down_weight)
+    mixed_rows, send_rows, placing, gates = front(arguments, capacity)
+    returned = moe(send_rows, gates, gate_weight, up_weight, down_weight)
     expert_out = lax.dot_general(
         placing.reshape(-1, tok_rows),
         returned.reshape(-1, width),

time: 118 us -> 114 us (0.966)
  Pallas kernels: 114 us -> 111 us
    pallas_call x1, Pallas kernels: 114 us -> 111 us  [layer(): pl.pallas_call(functools.partial(layer_kernel, len(arguments), len(front_...]
where the time goes in v4:
time: 114 us; the launch traced here: 113 us
  Pallas kernels  111 us (97%)
  local copies, waits for them, and re-layouts  1.88 us (2%)
    pallas_call x1, Pallas kernels, layer(): pl.pallas_call(functools.partial(layer_kernel, len(arguments), len(front_...  111 us

profile of v4, /device:TPU:16, one launch (start us, length us, event | category | flops | bytes accessed | tf_op | source)
XLA Modules:
  0.0 112.9 jit_solution(14049702717745995520)
XLA Ops:
  0.0 111.0 %layer.1 = bf16[128,2048]{1,0:T(8,128)(2,1)} custom-call(bf16[1024,256]{1,0:T(8,128)(2,1)} %refs_0_.1, bf16[1024,512]{1,0:T(8,128)(2,1)} %refs_1_.1, bf16[1024,512]{1,0:T(8,128)(2,1)} %refs_2_.1, f32[2]{0:T(128)} %refs_3_.1, bf16[4,2,32,2048]{3,2,1,0:T(8,128)(2,1)} %bitcast.8, bf16[128,2048]{1,0:T(8,128)(2,1)} %refs_5_.1, f32[1,2048]{1,0:T(1,128)} %bitcast.9, ...), custom_call_target="tpu_custom_call" | custom-call | tf_op jit(solution)/shard_map/layer/pallas_call | solution.py:1046
  111.0 1.9 %copy.16 = bf16[128,2048]{1,0:T(8,128)(2,1)} copy(bf16[128,2048]{1,0:T(8,128)(2,1)} %layer.1) | data formatting | bytes 1048576

commit v5 on v4

--- a/solution.py
+++ b/solution.py
@@ -265,7 +265,7 @@
     reaches = (last - z, z)
     lags = tuple(jnp.where(depth == 0, 0, 2 * depth + 1) for depth in (last - z, z))
 
-    spare = max(0, 2 * last - 3)
+    spare = max(0, 2 * last - 2)
 
     def step(k, carry):
         for j in range(near):
@@ -277,10 +277,12 @@
                     line(side, index, j).wait_recv()
                     forward(side, index, j)
                     across(index, j).start()
-
-                @pl.when(k == 2 * reaches[side])
-                def _(side=side, j=j):
+        for side in range(2):
+            @pl.when(k == jnp.maximum(2 * reaches[side] - 1, 0))
+            def _(side=side):
+                for j in range(near):
                     forward(side, z * 2 + 1, j)
+
         for side in range(2):
             i = k - lags[side]
 
@@ -484,278 +486,6 @@
         pl.semaphore_signal(barrier, inc=1, device_id={"tp": lax.rem(tp + shift, parts)})
     for peer in peers[1:]:
         pl.semaphore_signal(barrier, inc=1, device_id={"sp": peer})
-    pl.semaphore_wait(barrier, parts + groups - 2)
-
-    def line(side, home, half):
-        place = full.at[home * CORES + core, group, half]
-        return pltpu.make_async_remote_copy(
-            src_ref=place,
-            dst_ref=place,
-            send_sem=line_send.at[side, home, half],
-            recv_sem=line_recv.at[home, half],
-            device_id={"tp": sides[side][0]},
-        )
-
-    def plane(home, j, half, target, source):
-        place = full.at[home * CORES + core, source, half]
-        return pltpu.make_async_remote_copy(
-            src_ref=place,
-            dst_ref=place,
-            send_sem=plane_send.at[home, j, half],
-            recv_sem=plane_recv.at[home, j, half],
-            device_id={"sp": target},
-        )
-
-    def relay(home, half):
-        target, source = (peers[2], peers[1]) if half == 0 else (peers[1], peers[2])
-        return plane(home, 3, half, target, source)
-
-    def across(home):
-        place = full.at[home * CORES + core]
-        return pltpu.make_async_remote_copy(
-            src_ref=place,
-            dst_ref=place,
-            send_sem=core_send.at[home],
-            recv_sem=core_recv.at[home],
-            device_id={"tp": partner},
-        )
-
-    def across_part(home, part, half):
-        place = full.at[home * CORES + core, part, half]
-        return pltpu.make_async_remote_copy(
-            src_ref=place,
-            dst_ref=place,
-            send_sem=core_send.at[home],
-            recv_sem=core_recv.at[home],
-            device_id={"tp": partner},
-        )
-
-    def halo(side):
-        start = WINDOW if side == 0 else seq_rows
-        landing = WINDOW + seq_rows if side == 0 else 0
-        return pltpu.make_async_remote_copy(
-            src_ref=span.at[:, pl.ds(start, WINDOW)],
-            dst_ref=span.at[:, pl.ds(landing, WINDOW)],
-            send_sem=halo_send.at[side],
-            recv_sem=halo_recv.at[side],
-            device_id={"sp": lax.rem(group + (groups - 1 if side == 0 else 1), groups)},
-        )
-
-    def row_block(shift):
-        target = lax.rem(tp + shift, parts)
-        return pltpu.make_async_remote_copy(
-            src_ref=attended.at[target],
-            dst_ref=received.at[tp],
-            send_sem=row_send.at[shift],
-            recv_sem=row_recv.at[shift],
-            device_id={"tp": target},
-        )
-
-    def share(home):
-        return pltpu.make_async_remote_copy(
-            src_ref=prod.at[home, 1 - core],
-            dst_ref=prod_pair.at[home],
-            send_sem=pair_send.at[home],
-            recv_sem=pair_recv.at[home],
-            device_id={"tp": partner},
-        )
-
-    def add_on(side, home):
-        slot = home if side == 1 else jnp.where(home == z - 1, length, home)
-        return pltpu.make_async_remote_copy(
-            src_ref=prod.at[home, core],
-            dst_ref=prod_inc.at[slot],
-            send_sem=sum_send.at[home],
-            recv_sem=sum_recv.at[slot],
-            device_id={"tp": sides[side][0]},
-        )
-
-    def added(slot):
-        return pltpu.make_async_remote_copy(
-            src_ref=prod_inc.at[slot],
-            dst_ref=prod_inc.at[slot],
-            send_sem=sum_send.at[0],
-            recv_sem=sum_recv.at[slot],
-            device_id={"tp": partner},
-        )
-
-    def pass_on(side, home):
-        share(home).wait_recv()
-
-        @pl.when(sides[1 - side][1])
-        def _():
-            added(home).wait_recv()
-
-        prod[home, core] = (
-            prod[home, core].astype(jnp.float32)
-            + prod_pair[home].astype(jnp.float32)
-            + prod_inc[home].astype(jnp.float32)
-        ).astype(prod.dtype)
-        add_on(side, home).start()
-
-    mirrored = [partner_slot(group, -j % groups, groups) for j in range(groups)]
-
-    def gate_swap(j):
-        return pltpu.make_async_remote_copy(
-            src_ref=gate_rows.at[mirrored[j]],
-            dst_ref=gates_ref.at[tp, j],
-            send_sem=gate_send.at[j],
-            recv_sem=gate_recv.at[j],
-            device_id={"sp": mirrored[j]},
-        )
-
-    def gate_block(shift):
-        place = gates_ref.at[tp]
-        return pltpu.make_async_remote_copy(
-            src_ref=place,
-            dst_ref=place,
-            send_sem=gates_send.at[shift],
-            recv_sem=gates_recv.at[shift],
-            device_id={"tp": lax.rem(tp + shift, parts)},
-        )
-
-    inward = (group > 0, group < groups - 1)
-    loads[0].wait()
-    for half in range(halves):
-        for side in range(2):
-            @pl.when(sides[side][1])
-            def _(side=side, half=half):
-                line(side, z, half).start()
-    loads[1].wait()
-    loads[2].wait()
-    for side in range(2):
-        @pl.when(inward[side])
-        def _(side=side):
-            halo(side).start()
-    across(z).start()
-    loads[3].wait()
-    loads[4].wait()
-
-    def attend(n, carry):
-        b = jnp.where(n < blocks - 2, n + 1, jnp.where(n == blocks - 2, 0, blocks - 1))
-
-        @pl.when(n == blocks - 2)
-        def _():
-            for side in range(2):
-                @pl.when(inward[1 - side])
-                def _(side=side):
-                    halo(side).wait_recv()
-
-        start = pl.multiple_of(b * BLOCK, BLOCK)
-        wide = query[pl.ds(start, BLOCK), :]
-        tall = jnp.concatenate(
-            [wide[:, h * HEAD_DIM : (h + 1) * HEAD_DIM] for h in range(heads_dev)], axis=0
-        )
-        reach = BLOCK + 2 * WINDOW
-        keys = span[0, pl.ds(start, reach), :]
-        values = span[1, pl.ds(start, reach), :]
-        scores = lax.dot_general(
-            tall, keys, (((1,), (1,)), ((), ())), preferred_element_type=jnp.float32
-        ) * HEAD_DIM ** (-0.5)
-        shape = (heads_dev * BLOCK, reach)
-        row = lax.broadcasted_iota(jnp.int32, shape, 0) % BLOCK
-        column = lax.broadcasted_iota(jnp.int32, shape, 1)
-        place = column + (group * seq_rows + b * BLOCK - WINDOW)
-        inside = (
-            (column >= row) & (column <= row + 2 * WINDOW)
-            & (place >= 0) & (place < seq_rows * groups)
-        )
-        scores = jnp.where(inside, scores, NEG_BIG)
-        which = lax.broadcasted_iota(jnp.int32, (heads_dev * BLOCK, 1), 0) // BLOCK
-        sink = jnp.zeros((heads_dev * BLOCK, 1), jnp.float32)
-        for h in range(heads_dev):
-            sink = jnp.where(which == h, sink_ref[h], sink)
-        top = jnp.maximum(jnp.max(scores, axis=1, keepdims=True), sink)
-        terms = jnp.exp(scores - top)
-        mass = jnp.sum(terms, axis=1, keepdims=True) + jnp.exp(sink - top)
-        weight = (terms / mass).astype(jnp.bfloat16)
-        result = jnp.dot(weight, values, preferred_element_type=jnp.float32).astype(jnp.bfloat16)
-        attended[b] = jnp.concatenate(
-            [result[h * BLOCK : (h + 1) * BLOCK] for h in range(heads_dev)], axis=1
-        )
-        return carry
-
-
-    def homes(i):
-        return ((z + 1 + i, z + 1 + i <= last), (z - 1 - i, z - 1 - i >= 0))
-
-    def spread_half(i, half):
-        for side in range(2):
-            home, live = homes(i)[side]
-
-            @pl.when(live)
-            def _(side=side, home=home):
-                line(side, home, half).wait_recv()
-
-                @pl.when(sides[side][1])
-                def _():
-                    line(side, home, half).start()
-
-                across_part(home, group, half).start()
-                if not relayed:
-                    for j in range(1, groups):
-                        plane(home, j, half, peers[j], group).start()
-                elif half == 0:
-                    plane(home, 1, 0, peers[1], group).start()
-                else:
-                    plane(home, 2, 1, peers[2], group).start()
-                    plane(home, 1, 1, peers[1], group).start()
-                    plane(home, 2, 0, peers[2], group).start()
-
-    def relay_half(i, half):
-        for side in range(2):
-            home, live = homes(i)[side]
-
-            @pl.when(live)
-            def _(home=home):
-                plane(home, 1 + half, half, peers[1], group).wait_recv()
-                relay(home, half).start()
-                across_part(home, peers[1 + half], half).start()
-
-    def multiply(home, carry):
-        lhs = jnp.concatenate([attended[home * CORES + c] for c in range(CORES)], axis=0)
-        part = jnp.dot(
-            lhs, own_weight[...].reshape(-1, summed), preferred_element_type=jnp.float32
-        )
-        prod[home] = part.astype(prod.dtype).reshape(CORES, -1, summed)
-        share(home).start()
-        return carry
-
-    depths = (last - z, z)
-
-    def add_step(r):
-        for side in range(2):
-            event = r - (depths[side] - 1)
-            home = last - event if side == 1 else event
-
-            @pl.when((depths[side] > 0) & (event >= 0) & (event < depths[1 - side]))
-            def _(side=side, home=home):
-                pass_on(side, home)
-
-    def spread(i):
-        for half in range(halves):
-            spread_half(i, half)
-        if relayed:
-            for half in range(halves):
-                relay_half(i, half)
-
-    def first_sums():
-        for side in range(2):
-            @pl.when(depths[side] == 0)
-            def _(side=side):
-                for event in range(last):
-                    pass_on(side, last - event if side == 1 else event)
-
-    def send_rows():
-        for shift in range(1, parts):
-            row_block(shift).start()
-
-    lax.fori_loop(0, blocks, attend, 0)
-    received[tp] = attended[tp]
-    send_rows()
-    lax.fori_loop(0, length, multiply, 0)
-    spread(0)
-    first_sums()
     capacity = rows_ref.shape[1]
     slots = groups * capacity
     tok_rows = residual.shape[0]
@@ -787,9 +517,288 @@
             tail.astype(jnp.bfloat16), (chosen_slot == slot_row).astype(jnp.bfloat16),
             (((1,), (1,)), ((), ())), preferred_element_type=jnp.float32,
         ).astype(gate_rows.dtype)
+    pl.semaphore_wait(barrier, parts + groups - 2)
+
+    def line(side, home, half):
+        place = full.at[home * CORES + core, group, half]
+        return pltpu.make_async_remote_copy(
+            src_ref=place,
+            dst_ref=place,
+            send_sem=line_send.at[side, home, half],
+            recv_sem=line_recv.at[home, half],
+            device_id={"tp": sides[side][0]},
+        )
+
+    def plane(home, j, half, target, source):
+        place = full.at[home * CORES + core, source, half]
+        return pltpu.make_async_remote_copy(
+            src_ref=place,
+            dst_ref=place,
+            send_sem=plane_send.at[home, j, half],
+            recv_sem=plane_recv.at[home, j, half],
+            device_id={"sp": target},
+        )
+
+    def relay(home, half):
+        target, source = (peers[2], peers[1]) if half == 0 else (peers[1], peers[2])
+        return plane(home, 3, half, target, source)
+
+    def across(home):
+        place = full.at[home * CORES + core]
+        return pltpu.make_async_remote_copy(
+            src_ref=place,
+            dst_ref=place,
+            send_sem=core_send.at[home],
+            recv_sem=core_recv.at[home],
+            device_id={"tp": partner},
+        )
+
+    def across_part(home, part, half):
+        place = full.at[home * CORES + core, part, half]
+        return pltpu.make_async_remote_copy(
+            src_ref=place,
+            dst_ref=place,
+            send_sem=core_send.at[home],
+            recv_sem=core_recv.at[home],
+            device_id={"tp": partner},
+        )
+
+    def halo(side):
+        start = WINDOW if side == 0 else seq_rows
+        landing = WINDOW + seq_rows if side == 0 else 0
+        return pltpu.make_async_remote_copy(
+            src_ref=span.at[:, pl.ds(start, WINDOW)],
+            dst_ref=span.at[:, pl.ds(landing, WINDOW)],
+            send_sem=halo_send.at[side],
+            recv_sem=halo_recv.at[side],
+            device_id={"sp": lax.rem(group + (groups - 1 if side == 0 else 1), groups)},
+        )
+
+    def row_block(shift):
+        target = lax.rem(tp + shift, parts)
+        return pltpu.make_async_remote_copy(
+            src_ref=attended.at[target],
+            dst_ref=received.at[tp],
+            send_sem=row_send.at[shift],
+            recv_sem=row_recv.at[shift],
+            device_id={"tp": target},
+        )
+
+    def share(home):
+        return pltpu.make_async_remote_copy(
+            src_ref=prod.at[home, 1 - core],
+            dst_ref=prod_pair.at[home],
+            send_sem=pair_send.at[home],
+            recv_sem=pair_recv.at[home],
+            device_id={"tp": partner},
+        )
+
+    def add_on(side, home):
+        slot = home if side == 1 else jnp.where(home == z - 1, length, home)
+        return pltpu.make_async_remote_copy(
+            src_ref=prod.at[home, core],
+            dst_ref=prod_inc.at[slot],
+            send_sem=sum_send.at[home],
+            recv_sem=sum_recv.at[slot],
+            device_id={"tp": sides[side][0]},
+        )
+
+    def added(slot):
+        return pltpu.make_async_remote_copy(
+            src_ref=prod_inc.at[slot],
+            dst_ref=prod_inc.at[slot],
+            send_sem=sum_send.at[0],
+            recv_sem=sum_recv.at[slot],
+            device_id={"tp": partner},
+        )
+
+    def pass_on(side, home):
+        share(home).wait_recv()
+
+        @pl.when(sides[1 - side][1])
+        def _():
+            added(home).wait_recv()
+
+        prod[home, core] = (
+            prod[home, core].astype(jnp.float32)
+            + prod_pair[home].astype(jnp.float32)
+            + prod_inc[home].astype(jnp.float32)
+        ).astype(prod.dtype)
+        add_on(side, home).start()
+
+    mirrored = [partner_slot(group, -j % groups, groups) for j in range(groups)]
+
+    def gate_swap(j):
+        return pltpu.make_async_remote_copy(
+            src_ref=gate_rows.at[mirrored[j]],
+            dst_ref=gates_ref.at[tp, j],
+            send_sem=gate_send.at[j],
+            recv_sem=gate_recv.at[j],
+            device_id={"sp": mirrored[j]},
+        )
+
+    def gate_block(shift):
+        place = gates_ref.at[tp]
+        return pltpu.make_async_remote_copy(
+            src_ref=place,
+            dst_ref=place,
+            send_sem=gates_send.at[shift],
+            recv_sem=gates_recv.at[shift],
+            device_id={"tp": lax.rem(tp + shift, parts)},
+        )
+
+    inward = (group > 0, group < groups - 1)
+    loads[0].wait()
+    for half in range(halves):
+        for side in range(2):
+            @pl.when(sides[side][1])
+            def _(side=side, half=half):
+                line(side, z, half).start()
     gates_ref[tp, 0] = gate_rows[group]
     for j in range(1, groups):
         gate_swap(j).start()
+    loads[1].wait()
+    loads[2].wait()
+    for side in range(2):
+        @pl.when(inward[side])
+        def _(side=side):
+            halo(side).start()
+    across(z).start()
+    loads[3].wait()
+    loads[4].wait()
+
+    def attend(n, carry):
+        b = jnp.where(n < blocks - 2, n + 1, jnp.where(n == blocks - 2, 0, blocks - 1))
+
+        @pl.when(n == blocks - 2)
+        def _():
+            for side in range(2):
+                @pl.when(inward[1 - side])
+                def _(side=side):
+                    halo(side).wait_recv()
+
+        start = pl.multiple_of(b * BLOCK, BLOCK)
+        wide = query[pl.ds(start, BLOCK), :]
+        tall = jnp.concatenate(
+            [wide[:, h * HEAD_DIM : (h + 1) * HEAD_DIM] for h in range(heads_dev)], axis=0
+        )
+        reach = BLOCK + 2 * WINDOW
+        keys = span[0, pl.ds(start, reach), :]
+        values = span[1, pl.ds(start, reach), :]
+        scores = lax.dot_general(
+            tall, keys, (((1,), (1,)), ((), ())), preferred_element_type=jnp.float32
+        ) * HEAD_DIM ** (-0.5)
+        shape = (heads_dev * BLOCK, reach)
+        row = lax.broadcasted_iota(jnp.int32, shape, 0) % BLOCK
+        column = lax.broadcasted_iota(jnp.int32, shape, 1)
+        place = column + (group * seq_rows + b * BLOCK - WINDOW)
+        inside = (
+            (column >= row) & (column <= row + 2 * WINDOW)
+            & (place >= 0) & (place < seq_rows * groups)
+        )
+        scores = jnp.where(inside, scores, NEG_BIG)
+        which = lax.broadcasted_iota(jnp.int32, (heads_dev * BLOCK, 1), 0) // BLOCK
+        sink = jnp.zeros((heads_dev * BLOCK, 1), jnp.float32)
+        for h in range(heads_dev):
+            sink = jnp.where(which == h, sink_ref[h], sink)
+        top = jnp.maximum(jnp.max(scores, axis=1, keepdims=True), sink)
+        terms = jnp.exp(scores - top)
+        mass = jnp.sum(terms, axis=1, keepdims=True) + jnp.exp(sink - top)
+        weight = (terms / mass).astype(jnp.bfloat16)
+        result = jnp.dot(weight, values, preferred_element_type=jnp.float32).astype(jnp.bfloat16)
+        attended[b] = jnp.concatenate(
+            [result[h * BLOCK : (h + 1) * BLOCK] for h in range(heads_dev)], axis=1
+        )
+        return carry
+
+
+    def homes(i):
+        return ((z + 1 + i, z + 1 + i <= last), (z - 1 - i, z - 1 - i >= 0))
+
+    def spread_half(i, half):
+        for side in range(2):
+            home, live = homes(i)[side]
+
+            @pl.when(live)
+            def _(side=side, home=home):
+                line(side, home, half).wait_recv()
+
+                @pl.when(sides[side][1])
+                def _():
+                    line(side, home, half).start()
+
+                across_part(home, group, half).start()
+                if not relayed:
+                    for j in range(1, groups):
+                        plane(home, j, half, peers[j], group).start()
+                elif half == 0:
+                    plane(home, 1, 0, peers[1], group).start()
+                else:
+                    plane(home, 2, 1, peers[2], group).start()
+                    plane(home, 1, 1, peers[1], group).start()
+                    plane(home, 2, 0, peers[2], group).start()
+
+    def relay_half(i, half):
+        for side in range(2):
+            home, live = homes(i)[side]
+
+            @pl.when(live)
+            def _(home=home):
+                plane(home, 1 + half, half, peers[1], group).wait_recv()
+                relay(home, half).start()
+                across_part(home, peers[1 + half], half).start()
+
+    def multiply(home, carry):
+        lhs = jnp.concatenate([attended[home * CORES + c] for c in range(CORES)], axis=0)
+        part = jnp.dot(
+            lhs, own_weight[...].reshape(-1, summed), preferred_element_type=jnp.float32
+        )
+        prod[home] = part.astype(prod.dtype).reshape(CORES, -1, summed)
+        share(home).start()
+        return carry
+
+    depths = (last - z, z)
+
+    def add_step(r):
+        for side in range(2):
+            event = r - (depths[side] - 1)
+            home = last - event if side == 1 else event
+
+            @pl.when((depths[side] > 0) & (event >= 0) & (event < depths[1 - side]))
+            def _(side=side, home=home):
+                pass_on(side, home)
+
+    def spread(i):
+        for half in range(halves):
+            spread_half(i, half)
+        if relayed:
+            for half in range(halves):
+                relay_half(i, half)
+
+    def first_sums():
+        for side in range(2):
+            @pl.when(depths[side] == 0)
+            def _(side=side):
+                for event in range(last):
+                    pass_on(side, last - event if side == 1 else event)
+
+    def send_rows(reach):
+        if 1 in reach:
+            row_block(lax.rem(partner - tp + parts, parts)).start()
+        for distance in reach:
+            for target in (z + distance, z - distance):
+                @pl.when((target >= 0) & (target <= last))
+                def _(target=target):
+                    for c in range(CORES):
+                        row_block(lax.rem(target * CORES + c - tp + parts, parts)).start()
+
+    lax.fori_loop(0, blocks, attend, 0)
+    received[tp] = attended[tp]
+    send_rows(range(2, length))
+    lax.fori_loop(0, length, multiply, 0)
+    spread(0)
+    first_sums()
+    send_rows(range(1, 2))
     for i in range(1, last):
         add_step(i - 1)
         spread(i)

time: 114 us -> 113 us (level)
  no operation moved by 1% of the time
where the time goes in v5:
time: 113 us
  Pallas kernels  111 us (98%)
  local copies, waits for them, and re-layouts  1.88 us (2%)
    pallas_call x1, Pallas kernels, layer(): pl.pallas_call(functools.partial(layer_kernel, len(arguments), len(front_...  111 us

profile of v5, /device:TPU:16, one launch (start us, length us, event | category | flops | bytes accessed | tf_op | source)
XLA Modules:
  0.0 112.7 jit_solution(17979472477845504662)
XLA Ops:
  0.0 110.8 %layer.1 = bf16[128,2048]{1,0:T(8,128)(2,1)} custom-call(bf16[1024,256]{1,0:T(8,128)(2,1)} %refs_0_.1, bf16[1024,512]{1,0:T(8,128)(2,1)} %refs_1_.1, bf16[1024,512]{1,0:T(8,128)(2,1)} %refs_2_.1, f32[2]{0:T(128)} %refs_3_.1, bf16[4,2,32,2048]{3,2,1,0:T(8,128)(2,1)} %bitcast.8, bf16[128,2048]{1,0:T(8,128)(2,1)} %refs_5_.1, f32[1,2048]{1,0:T(1,128)} %bitcast.9, ...), custom_call_target="tpu_custom_call" | custom-call | tf_op jit(solution)/shard_map/layer/pallas_call | solution.py:1055
  110.9 1.9 %copy.16 = bf16[128,2048]{1,0:T(8,128)(2,1)} copy(bf16[128,2048]{1,0:T(8,128)(2,1)} %layer.1) | data formatting | bytes 1048576

commit v6 on v5

--- a/solution.py
+++ b/solution.py
@@ -704,8 +704,9 @@
         top = jnp.maximum(jnp.max(scores, axis=1, keepdims=True), sink)
         terms = jnp.exp(scores - top)
         mass = jnp.sum(terms, axis=1, keepdims=True) + jnp.exp(sink - top)
-        weight = (terms / mass).astype(jnp.bfloat16)
-        result = jnp.dot(weight, values, preferred_element_type=jnp.float32).astype(jnp.bfloat16)
+        result = (
+            jnp.dot(terms.astype(jnp.bfloat16), values, preferred_element_type=jnp.float32) / mass
+        ).astype(jnp.bfloat16)
         attended[b] = jnp.concatenate(
             [result[h * BLOCK : (h + 1) * BLOCK] for h in range(heads_dev)], axis=1
         )

time: 113 us -> 113 us (level)
  no operation moved by 1% of the time
where the time goes in v6:
time: 113 us
  Pallas kernels  111 us (98%)
  local copies, waits for them, and re-layouts  1.88 us (2%)
    pallas_call x1, Pallas kernels, layer(): pl.pallas_call(functools.partial(layer_kernel, len(arguments), len(front_...  111 us

profile of v6, /device:TPU:16, one launch (start us, length us, event | category | flops | bytes accessed | tf_op | source)
XLA Modules:
  0.0 112.9 jit_solution(11167602447979446406)
XLA Ops:
  0.0 111.0 %layer.1 = bf16[128,2048]{1,0:T(8,128)(2,1)} custom-call(bf16[1024,256]{1,0:T(8,128)(2,1)} %refs_0_.1, bf16[1024,512]{1,0:T(8,128)(2,1)} %refs_1_.1, bf16[1024,512]{1,0:T(8,128)(2,1)} %refs_2_.1, f32[2]{0:T(128)} %refs_3_.1, bf16[4,2,32,2048]{3,2,1,0:T(8,128)(2,1)} %bitcast.8, bf16[128,2048]{1,0:T(8,128)(2,1)} %refs_5_.1, f32[1,2048]{1,0:T(1,128)} %bitcast.9, ...), custom_call_target="tpu_custom_call" | custom-call | tf_op jit(solution)/shard_map/layer/pallas_call | solution.py:1056
  111.0 1.9 %copy.16 = bf16[128,2048]{1,0:T(8,128)(2,1)} copy(bf16[128,2048]{1,0:T(8,128)(2,1)} %layer.1) | data formatting | bytes 1048576
